TPU v7x, 512 devices: a whole 4x4x16 slice. The times are simulated.
512 devices in a mesh: sp: 64 (over z, y), tp: 8 (over x, core).
Axes of the slice: x: 4, y: 4, z: 16, core: 2. Of those that a mesh axis runs over, the one named last changes fastest.
Arguments:
- tokens: bfloat16 [16384, 2048], P('sp', 'tp'), may hold values from -6 to 6
- norm_gain: float32 [2048], replicated, may hold values from 0.1 to 1.9
- query_weight: bfloat16 [2048, 1024], P(None, 'tp'), may hold values from -0.18782524 to 0.18782524
- key_weight: bfloat16 [2048, 1024], P(None, 'tp'), may hold values from -0.18782524 to 0.18782524
- value_weight: bfloat16 [2048, 1024], P(None, 'tp'), may hold values from -0.125 to 0.125
- gate_weight: bfloat16 [2048, 1024], P(None, 'tp'), may hold values from -0.125 to 0.125
- outer_weight: bfloat16 [2048, 1024], P(None, 'tp'), may hold values from -0.125 to 0.125
- inner_weight: bfloat16 [2048, 1024], P(None, 'tp'), may hold values from -0.125 to 0.125
- signal_weight: bfloat16 [2048, 1024], P(None, 'tp'), may hold values from -0.125 to 0.125
- conv_taps: float32 [3, 1024], P(None, 'tp'), may hold values from -3.5 to 3.5
- lambdas: float32 [8], P('tp'), may hold values from 0.3 to 0.8
- head_gain: float32 [1024], P('tp'), may hold values from 0.1 to 1.9
- attn_out_weight: bfloat16 [1024, 2048], P('tp'), may hold values from -0.125 to 0.125
- conv_out_weight: bfloat16 [1024, 2048], P('tp'), may hold values from -0.125 to 0.125
Outputs:
- mixed: bfloat16 [16384, 2048], P(('sp', 'tp'))
- log_totals: float32 [8, 2, 16384], P('tp', None, 'sp')
All inputs are finite; a program needn't handle non-finite values.
Results may differ from a plain program's by a relative error of at most 0.014.
Values may be sent and summed in bfloat16 or wider, within the bound.
No kernel may reach another device: no remote copies, remote signals or barrier semaphores. Data moves between devices by JAX's collectives and lax.ppermute only.
A program may use at most 64 MiB of HBM per device.

v0:
```python
import jax
import jax.numpy as jnp
from jax import lax
from jax.sharding import PartitionSpec as P


def sent_to_all(shard, axis):
    copies = jnp.broadcast_to(shard, (lax.axis_size(axis), *shard.shape))
    return lax.all_to_all(copies, axis, split_axis=0, concat_axis=0, tiled=True)


def joined_along(tiles, dim):
    lengths = list(tiles.shape[1:])
    lengths[dim] *= tiles.shape[0]
    return jnp.moveaxis(tiles, 0, dim).reshape(lengths)


def gather_directly(shard, axis, dim):
    tiles = sent_to_all(shard, axis)
    return joined_along(tiles, dim)


def sent_together(arrays, axis, dim, along):
    ends, at = ([], 0)
    for a in arrays[:-1]:
        at += a.shape[along]
        ends.append(at)
    both = jnp.concatenate(arrays, axis=along)
    return tuple(jnp.split(lax.all_gather(both, axis, axis=dim, tiled=True), ends, axis=along))


def passed_along(shard, axis, by):
    count = lax.axis_size(axis)
    pairs = [(i, i + by) for i in range(count) if 0 <= i + by < count]
    return lax.ppermute(shard, axis, pairs)


def in_blocks(shard, dim, count):
    before, after = (shard.shape[:dim], shard.shape[dim + 1 :])
    return jnp.moveaxis(shard.reshape(*before, count, -1, *after), dim, 0)


def sent_and_summed(shard, axis, dim):
    count = lax.axis_size(axis)
    tiles = lax.all_to_all(in_blocks(shard, dim, count), axis, 0, 0, tiled=True)
    return jnp.sum(tiles.astype(jnp.float32), axis=0)


def per_device(
    tokens,
    norm_gain,
    query_weight,
    key_weight,
    value_weight,
    gate_weight,
    outer_weight,
    inner_weight,
    signal_weight,
    conv_taps,
    lambdas,
    head_gain,
    attn_out_weight,
    conv_out_weight,
):
    row_count = tokens.shape[0]
    width = norm_gain.shape[0]
    weights = [
        query_weight,
        key_weight,
        value_weight,
        gate_weight,
        outer_weight,
        inner_weight,
        signal_weight,
    ]
    splits = []
    running = 0
    for weight in weights[:-1]:
        running = running + weight.shape[1]
        splits.append(running)
    joined = jnp.concatenate(weights, axis=1)
    empty = jnp.zeros((row_count, joined.shape[1]), jnp.float32)
    piece = gather_directly(tokens, "tp", 1)
    summed = empty
    piece_f = piece.astype(jnp.float32)
    normed_piece = (piece.astype(jnp.float32) * norm_gain).astype(jnp.bfloat16)
    raw = jnp.dot(normed_piece, joined, preferred_element_type=jnp.float32)
    squares = jnp.sum(piece_f * piece_f, axis=-1)
    scale = lax.rsqrt(squares / width + 1e-06)
    projected = (raw * scale[:, None]).astype(jnp.bfloat16)
    query, key, value, attn_gate, outer, inner, signal = jnp.split(projected, splits, axis=1)
    head_count = lambdas.shape[0]
    key_size = query_weight.shape[1] // (head_count * 2)
    value_size = value_weight.shape[1] // head_count
    score_scale = key_size ** (-0.5)
    own_index = lax.axis_index("sp")
    local_pos = jnp.arange(row_count, dtype=jnp.int32)
    query_parts = [query]
    position_parts = [own_index * row_count + local_pos]
    query_parts = [
        segment.reshape(segment.shape[0], head_count, 2, key_size) for segment in query_parts
    ]

    def absorb(current, query_rows, row_pos, key_block, value_block, key_pos):
        running_max, summed, accum = current
        score = (
            jnp.einsum("qhmd,khmd->hmqk", query_rows, key_block, preferred_element_type=jnp.float32)
            * score_scale
        )
        visible = row_pos[:, None] >= key_pos[None, :]
        masked = jnp.where(visible, score, -1e30)
        new_max = jnp.maximum(running_max, jnp.max(masked, axis=-1, keepdims=True))
        weights_now = jnp.where(visible, jnp.exp(masked - new_max), 0.0)
        factor = jnp.exp(running_max - new_max)
        summed = summed * factor + jnp.sum(weights_now, axis=-1, keepdims=True)
        accum = accum * factor + jnp.einsum(
            "hmqk,khd->hmqd",
            weights_now.astype(jnp.bfloat16),
            value_block,
            preferred_element_type=jnp.float32,
        )
        return (new_max, summed, accum)

    def fresh(rows):
        return (
            jnp.full((head_count, 2, rows, 1), -1e30, jnp.float32),
            jnp.zeros((head_count, 2, rows, 1), jnp.float32),
            jnp.zeros((head_count, 2, rows, value_size), jnp.float32),
        )

    start_states = tuple((fresh(segment.shape[0]) for segment in query_parts))
    carry = start_states
    key_piece, value_piece = sent_together((key, value), "sp", 0, 1)
    length = key_piece.shape[0]
    block_len = 512
    key_blocks = key_piece.reshape(length // block_len, block_len, head_count, 2, key_size)
    value_blocks = value_piece.reshape(length // block_len, block_len, head_count, value_size)

    def one_block(states, item):
        key_block, value_block, block_id = item
        first_key = block_id * block_len
        key_pos = first_key + jnp.arange(block_len, dtype=jnp.int32)
        updated = []
        for current, query_rows, row_pos in zip(states, query_parts, position_parts):

            def compute(held, query_rows=query_rows, row_pos=row_pos):
                return absorb(held, query_rows, row_pos, key_block, value_block, key_pos)

            def unchanged(held):
                return held

            updated.append(
                lax.cond(first_key <= row_pos[row_pos.shape[0] - 1], compute, unchanged, current)
            )
        return (tuple(updated), None)

    carry, _ = lax.scan(
        one_block,
        carry,
        (key_blocks, value_blocks, jnp.arange(length // block_len, dtype=jnp.int32)),
    )
    states = carry
    running_max = jnp.concatenate([held[0] for held in states], axis=2)
    summed = jnp.concatenate([held[1] for held in states], axis=2)
    accum = jnp.concatenate([held[2] for held in states], axis=2)
    mapped = accum / summed
    diff = mapped[:, 0] - lambdas[:, None, None] * mapped[:, 1]
    log_totals = jnp.log(summed[..., 0]) + running_max[..., 0]
    diff = jnp.transpose(diff, (1, 0, 2))
    normed = (
        diff
        * lax.rsqrt(jnp.mean(diff * diff, axis=-1, keepdims=True) + 1e-05)
        * head_gain.reshape(head_count, value_size)
    )
    normed = normed.reshape(row_count, head_count * value_size)
    head_out = (normed * jax.nn.silu(attn_gate.astype(jnp.float32))).astype(jnp.bfloat16)
    taps = conv_taps.shape[0]
    inner_sig = (inner.astype(jnp.float32) * signal.astype(jnp.float32)).astype(jnp.bfloat16)
    before = passed_along(inner_sig[row_count - (taps - 1) :], "sp", 1)
    extended = jnp.concatenate([before, inner_sig], axis=0).astype(jnp.float32)
    convolved = jnp.zeros((row_count, inner_sig.shape[1]), jnp.float32)
    for position in range(taps):
        convolved = convolved + conv_taps[position] * extended[position : position + row_count]
    conv_out = (outer.astype(jnp.float32) * convolved).astype(jnp.bfloat16)
    mixed = sent_and_summed(
        (
            jnp.dot(head_out, attn_out_weight, preferred_element_type=jnp.float32)
            + jnp.dot(conv_out, conv_out_weight, preferred_element_type=jnp.float32)
        ).astype(jnp.bfloat16),
        "tp",
        0,
    )
    return (mixed.astype(jnp.bfloat16), log_totals)


def solution(mesh):
    placed = (
        P("sp", "tp"),
        P(),
        P(None, "tp"),
        P(None, "tp"),
        P(None, "tp"),
        P(None, "tp"),
        P(None, "tp"),
        P(None, "tp"),
        P(None, "tp"),
        P(None, "tp"),
        P("tp"),
        P("tp"),
        P("tp", None),
        P("tp", None),
    )
    return jax.shard_map(
        per_device,
        mesh=mesh,
        in_specs=placed,
        out_specs=(P(("sp", "tp"), None), P("tp", None, "sp")),
        check_vma=False,
    )
```

profile of v0, /device:TPU:480, one launch (start us, length us, event | category | flops | bytes accessed | tf_op | source)
XLA Modules:
  0.0 432.5 jit_solution(13000434036668571965)
XLA Ops:
  9.4 4.3 all-to-all-start
  21.1 8.6 %all-to-all-done = bf16[8,256,256]{1,2,0:T(8,128)(2,1)S(1)} async-done(((bf16[8,256,256]{1,2,0:T(8,128)(2,1)}), bf16[8,256,256]{1,2,0:T(8,128)(2,1)S(1)}, u32[]{:S(2)}, u32[]{:S(2)}) %all-to-all-start) | async-done | bytes 1048608 | tf_op jit(solution)/shard_map/all_to_all | solution.py:9
  30.3 3.3 fusion.20
  34.4 3.5 collective-permute-start
  38.7 3.3 collective-permute-done
  42.0 144.4 %all-gather.2.cloned.1.call-done = bf16[16384,256]{1,0:T(8,128)(2,1)} async-done(((bf16[256,256]{1,0:T(8,128)(2,1)}), bf16[16384,256]{1,0:T(8,128)(2,1)}) %all-gather.2.cloned.1.call-update) | async-done | bytes 8388624 | tf_op jit(solution)/shard_map/all_gather | solution.py:29
  186.4 5.7 %fusion.46 = (bf16[16384,128]{1,0:T(8,128)(2,1)}, bf16[16384,128]{1,0:T(8,128)(2,1)}) fusion(bf16[16384,256]{1,0:T(8,128)(2,1)} %all-gather.2.cloned.1.call-done), kind=kLoop, calls=%fused_computation.79 | loop fusion | bytes 16777216 | tf_op jit(solution)/shard_map/split | solution.py:29
  192.1 14.7 %reshape.187 = bf16[32,512,1,2,64]{4,3,1,0,2:T(2,128)(2,1)} reshape(bf16[16384,128]{1,0:T(8,128)(2,1)} %get-tuple-element.187) | data formatting | bytes 8388608 | tf_op jit(solution)/shard_map/reshape | solution.py:136
  206.8 18.4 %copy.24 = bf16[32,512,1,2,64]{1,4,3,2,0:T(8,128)(2,1)} copy(bf16[32,512,1,2,64]{4,3,1,0,2:T(2,128)(2,1)} %reshape.187) | data formatting | bytes 8388608 | tf_op jit(solution)/shard_map/while | solution.py:157
  225.3 177.2 %while.14 = (s32[]{:T(128)}, f32[1,2,256,1]{2,1,3,0:T(2,128)S(1)}, f32[1,2,256,1]{2,1,3,0:T(2,128)S(1)}, f32[1,2,256,128]{3,2,1,0:T(8,128)S(1)}, s32[32]{0:T(128...) while((s32[]{:T(128)}, f32[1,2,256,1]{2,1,3,0:T(2,128)S(1)}, ...), condition=%wide.region_6.7_spmd, body=%wide.region_1.6_spmd.sunk | while | flops 103286784 | bytes 4565287 | solution.py:157
  227.8 3.1 conditional.2
  233.4 3.1 conditional.2
  239.0 3.1 conditional.2
  244.7 3.1 conditional.2
  250.3 3.1 conditional.2
  261.6 3.1 conditional.2
  267.2 3.1 conditional.2
  272.8 3.1 conditional.2
  289.7 3.1 conditional.2
  295.4 3.1 conditional.2
  312.3 3.1 conditional.2
  317.9 3.1 conditional.2
  323.5 3.1 conditional.2
  340.4 3.1 conditional.2
  346.1 3.1 conditional.2
  351.7 3.1 conditional.2
  368.6 3.1 conditional.2
  374.2 3.1 conditional.2
  379.9 3.1 conditional.2
  396.8 3.1 conditional.2
  404.9 4.1 all-to-all-start.1
  409.5 15.3 %all-to-all-done.1 = bf16[8,32,2048]{2,1,0:T(8,128)(2,1)S(1)} async-done(((bf16[8,32,2048]{2,1,0:T(8,128)(2,1)}), bf16[8,32,2048]{2,1,0:T(8,128)(2,1)S(1)}, u32[]{:S(2)}, u32[]{:S(2)}) %all-to-all-start.1) | async-done | bytes 1048608 | tf_op jit(solution)/shard_map/all_to_all | solution.py:45
  (411 shorter events, 182.1 us)
Async XLA Ops:
  7.2 395.6 %copy-start = (bf16[128,2048]{1,0:T(8,128)(2,1)S(1)}, bf16[128,2048]{1,0:T(8,128)(2,1)}, u32[]{:S(2)}) copy-start(bf16[128,2048]{1,0:T(8,128)(2,1)} %param.30) | copy-start | bytes 1572868
  7.2 6.6 %copy-start.2 = (bf16[2048,128]{1,0:T(8,128)(2,1)S(1)}, bf16[2048,128]{1,0:T(8,128)(2,1)}, u32[]{:S(2)}) copy-start(bf16[2048,128]{1,0:T(8,128)(2,1)} %param.20) | copy-start | bytes 1572868
  7.2 7.6 %copy-start.3 = (bf16[2048,128]{1,0:T(8,128)(2,1)S(1)}, bf16[2048,128]{1,0:T(8,128)(2,1)}, u32[]{:S(2)}) copy-start(bf16[2048,128]{1,0:T(8,128)(2,1)} %param.21) | copy-start | bytes 1572868
  7.2 8.4 %copy-start.4 = (bf16[2048,128]{1,0:T(8,128)(2,1)S(1)}, bf16[2048,128]{1,0:T(8,128)(2,1)}, u32[]{:S(2)}) copy-start(bf16[2048,128]{1,0:T(8,128)(2,1)} %param.22) | copy-start | bytes 1572868
  9.4 20.2 %all-to-all-start = ((bf16[8,256,256]{1,2,0:T(8,128)(2,1)}), bf16[8,256,256]{1,2,0:T(8,128)(2,1)S(1)}, u32[]{:S(2)}, u32[]{:S(2)}) async-start(bf16[8,256,256]{1,2,0:T(8,128)(2,1)} %broadcast_in_dim.43), calls=%async_computation | async-start | bytes 2097152 | tf_op jit(solution)/shard_map/all_to_all | solution.py:9
  13.7 172.7 %all-gather.2.cloned.1.call-start = ((), (), s32[]{:S(2)}) async-start(), calls=%async_computation.2 | async-start | bytes 8519680 | tf_op jit(solution)/shard_map/all_gather | solution.py:29
  13.8 4.6 %copy-start.5 = (bf16[2048,128]{1,0:T(8,128)(2,1)S(1)}, bf16[2048,128]{1,0:T(8,128)(2,1)}, u32[]{:S(2)}) copy-start(bf16[2048,128]{1,0:T(8,128)(2,1)} %param.24) | copy-start | bytes 1572868
  13.8 5.6 %copy-start.6 = (bf16[2048,128]{1,0:T(8,128)(2,1)S(1)}, bf16[2048,128]{1,0:T(8,128)(2,1)}, u32[]{:S(2)}) copy-start(bf16[2048,128]{1,0:T(8,128)(2,1)} %param.25) | copy-start | bytes 1572868
  13.8 6.4 %copy-start.7 = (bf16[2048,128]{1,0:T(8,128)(2,1)S(1)}, bf16[2048,128]{1,0:T(8,128)(2,1)}, u32[]{:S(2)}) copy-start(bf16[2048,128]{1,0:T(8,128)(2,1)} %param.26) | copy-start | bytes 1572868
  14.7 15.2 %copy-start.8 = (f32[2048]{0:T(1024)S(1)}, f32[2048]{0:T(1024)}, u32[]{:S(2)}) copy-start(f32[2048]{0:T(1024)} %param.19) | copy-start | bytes 24580
  30.3 4.1 copy-start.9
  34.4 7.6 %collective-permute-start = (bf16[2,128]{1,0:T(2,128)(2,1)S(1)}, bf16[2,128]{1,0:T(2,128)(2,1)S(1)}, u32[]{:S(2)}, u32[]{:S(2)}) collective-permute-start(bf16[2,128]{1,0:T(2,128)(2,1)S(1)} %slice.42), channel_id=1, source_target_pairs={{0,8},{8,16},{16,24},{24,32},{32,40},{40,48},{48,56},{56,64},{64,7... | collective-permute-start | bytes 1544 | tf_op jit(solution)/shard_map/ppermute | solution.py:35
  225.2 177.5 %copy-start.10 = (f32[128]{0:T(128)S(1)}, f32[128]{0:T(128)}, u32[]{:S(2)}) copy-start(f32[128]{0:T(128)} %param.29) | copy-start | bytes 1540
  402.4 1.0 copy-start.1
  404.9 20.0 %all-to-all-start.1 = ((bf16[8,32,2048]{2,1,0:T(8,128)(2,1)}), bf16[8,32,2048]{2,1,0:T(8,128)(2,1)S(1)}, u32[]{:S(2)}, u32[]{:S(2)}) async-start(bf16[8,32,2048]{2,1,0:T(8,128)(2,1)} %bitcast.23), calls=%async_computation.1 | async-start | bytes 2097152 | tf_op jit(solution)/shard_map/all_to_all | solution.py:45
Sparse Core Ops, SparseCore 0:
  34.5 151.8 all-gather.1
where the time goes:
time: 437 us; the launch traced here: 433 us
  waiting for transfers between devices  172 us (39%)
  local copies, waits for them, and re-layouts  87.7 us (20%)
  matrix products  87.5 us (20%)
  loops' own time  44.2 us (10%)
  between operations  14.9 us (3%)
  other arithmetic  14.7 us (3%)
  starting transfers between devices  11.9 us (3%)
    all_gather x1, waiting for transfers between devices, sent_together(): lax.all_gather(both, axis, axis=dim, tiled=True)  144 us
    dot_general x31, matrix products, absorb(): jnp.einsum('hmqk,khd->hmqd', weights_now.astype(jnp.bfloat16), value_bloc...  42.9 us
    another operation x1, loops' own time, per_device(): lax.scan(one_block, carry, (key_blocks, value_blocks, jnp.arange(length /...  42.4 us
    dot_general x31, matrix products, absorb(): jnp.einsum('qhmd,khmd->hmqk', query_rows, key_block, preferred_element_ty...  39.4 us
    slice x32, local copies, waits for them, and re-layouts, one_block(): row_pos[row_pos.shape[0] - 1]  19.4 us
    dynamic_slice x32, local copies, waits for them, and re-layouts, per_device(): lax.scan(one_block, carry, (key_blocks, value_blocks, jnp.arange(length /...  18.8 us
    while x1, local copies, waits for them, and re-layouts, per_device(): lax.scan(one_block, carry, (key_blocks, value_blocks, jnp.arange(length /...  18.4 us
    all_to_all x1, waiting for transfers between devices, sent_and_summed(): tiles = lax.all_to_all(in_blocks(shard, dim, count), axis, 0, 0, tiled=True)  15.3 us
  transfers between devices with their start and end apart: 4, of which 4 were waited for; matrix products, arithmetic and copies ran while one was open for 2% of the time, Pallas kernels for 0%

commit v1 on v0

v1 whole, which is shorter than its diff:
```python
import functools

import jax
import jax.numpy as jnp
from jax import lax
from jax.experimental import pallas as pl
from jax.experimental.pallas import tpu as pltpu
from jax.sharding import PartitionSpec as P

LOG2E = 1.4426950408889634
LN2 = 0.6931471805599453
HIDDEN = -1e30


def project_kernel(place, own, other, gain, qw, kw, vw, gw, ow, iw, sw, kv, q, gate, outer, insig, normed):
    count, rows, part = own.shape
    width = normed.shape[1]

    def spread(core):
        squares = jnp.zeros((rows, part), jnp.float32)
        for x in range(count):
            for ref, side in ((own, core), (other, 1 - core)):
                at = (2 * x + side) * part
                piece = ref[x].astype(jnp.float32)
                squares = squares + piece * piece
                normed[:, at : at + part] = (piece * gain[:, at : at + part]).astype(jnp.bfloat16)
        scale = lax.rsqrt(jnp.sum(squares, axis=-1, keepdims=True) / width + 1e-06)

        def project(weight, factor=None):
            raw = jnp.dot(normed[...], weight[...], preferred_element_type=jnp.float32)
            raw = raw * scale
            if factor is not None:
                raw = raw * factor
            return raw.astype(jnp.bfloat16)

        columns = kw.shape[1]
        kv[:, :columns] = project(kw)
        kv[:, columns:] = project(vw)
        q[...] = project(qw, LOG2E * (columns // 2) ** -0.5)
        insig[...] = (project(iw).astype(jnp.float32) * project(sw).astype(jnp.float32)).astype(jnp.bfloat16)
        outer[...] = project(ow)
        gate[...] = project(gw)

    for core in range(2):
        pl.when(place[0] == core)(functools.partial(spread, core))


def attend_kernel(place, q, kv, out):
    rows = q.shape[1]
    blocks, block_len, columns = kv.shape
    value_size = columns // 2
    key_size = value_size // 2
    step = pl.program_id(0)
    last = place[0]
    slot = place[1]
    ahead = (step - slot) * rows
    queries = q[0]
    ones = jnp.ones((block_len, value_size), jnp.bfloat16)

    def body(used):
        stats = []
        for m in range(2):
            query = queries[:, m * key_size : (m + 1) * key_size]
            scores = []
            for b in range(used):
                keys = kv[b][:, m * key_size : (m + 1) * key_size]
                scores.append(
                    lax.dot_general(query, keys, (((1,), (1,)), ((), ())), preferred_element_type=jnp.float32)
                )
            row = lax.broadcasted_iota(jnp.int32, (rows, block_len), 0)
            col = lax.broadcasted_iota(jnp.int32, (rows, block_len), 1)
            seen = row + ahead >= col
            scores[-1] = jnp.where(seen, scores[-1], HIDDEN)
            top = scores[0]
            for s in scores[1:]:
                top = jnp.maximum(top, s)
            top = jnp.max(top, axis=-1, keepdims=True)
            summed = jnp.zeros((rows, 2 * value_size), jnp.float32)
            for b in range(used):
                w = jnp.exp2(scores[b] - top)
                if b == used - 1:
                    w = jnp.where(seen, w, 0.0)
                values = jnp.concatenate([kv[b][:, value_size:], ones], axis=1)
                summed = summed + jnp.dot(w.astype(jnp.bfloat16), values, preferred_element_type=jnp.float32)
            total = summed[:, value_size:]
            some = total > 0.0
            safe = jnp.where(some, total, 1.0)
            out[0, :rows, m * value_size : (m + 1) * value_size] = (summed[:, :value_size] / safe).astype(
                jnp.bfloat16
            )
            stats.append(jnp.where(some, jnp.log2(safe) + top, HIDDEN))
        lane = lax.broadcasted_iota(jnp.int32, (rows, value_size), 1)
        spread = jnp.zeros((rows, value_size), jnp.float32)
        for m in range(2):
            rest = stats[m]
            for piece in range(3):
                rounded = rest.astype(jnp.bfloat16).astype(jnp.float32)
                spread = jnp.where(lane == 2 * piece + m, rounded, spread)
                rest = rest - rounded
        turned = jnp.transpose(spread)
        out[0, rows:, :] = turned[: out.shape[1] - rows].astype(jnp.bfloat16)

    for used in range(1, blocks + 1):
        pl.when(last == used - 1)(functools.partial(body, used))


def finish_kernel(lam, parts, gate, conv, head_gain, attn_w, conv_w, mixed, totals):
    count, _, columns = parts.shape
    rows = gate.shape[0]
    value_size = columns // 2
    tails = [parts[j, rows:, :].astype(jnp.float32) for j in range(count)]
    logs = [t[0:2] + t[2:4] + t[4:6] for t in tails]
    top = logs[0]
    for log in logs[1:]:
        top = jnp.maximum(top, log)
    shares = [jnp.exp2(log - top) for log in logs]
    total = shares[0]
    for share in shares[1:]:
        total = total + share
    totals[0] = (jnp.log2(total) + top) * LN2
    shares = [share / total for share in shares]
    pad = jnp.zeros((value_size - 2 * count, rows), jnp.float32)
    turned = jnp.transpose(jnp.concatenate([*shares, pad], axis=0))
    mapped = []
    for m in range(2):
        summed = jnp.zeros((rows, value_size), jnp.float32)
        for j in range(count):
            piece = parts[j, :rows, m * value_size : (m + 1) * value_size].astype(jnp.float32)
            summed = summed + turned[:, 2 * j + m : 2 * j + m + 1] * piece
        mapped.append(summed)
    diff = mapped[0] - lam[0] * mapped[1]
    norm = lax.rsqrt(jnp.mean(diff * diff, axis=-1, keepdims=True) + 1e-05)
    opened = gate[...].astype(jnp.float32)
    head = diff * norm * head_gain[...] * (opened / (1.0 + jnp.exp(-opened)))
    mixed[...] = (
        jnp.dot(head.astype(jnp.bfloat16), attn_w[...], preferred_element_type=jnp.float32)
        + jnp.dot(conv[...], conv_w[...], preferred_element_type=jnp.float32)
    ).astype(jnp.bfloat16)


VMEM = pl.BlockSpec(memory_space=pltpu.VMEM)
SMEM = pl.BlockSpec(memory_space=pltpu.SMEM)


def project(core, own, other, gain, weights):
    rows = own.shape[1]
    width = gain.shape[0]
    columns = weights[0].shape[1]
    narrow = jax.ShapeDtypeStruct((rows, columns), jnp.bfloat16)
    return pl.pallas_call(
        project_kernel,
        out_shape=(jax.ShapeDtypeStruct((rows, 2 * columns), jnp.bfloat16), narrow, narrow, narrow, narrow),
        in_specs=[SMEM] + [VMEM] * 10,
        out_specs=(VMEM,) * 5,
        scratch_shapes=[pltpu.VMEM((rows, width), jnp.bfloat16)],
        name="project",
    )(core.reshape(1), own, other, gain.reshape(1, width), *weights)


def attend(place, queries, kv, extra):
    count, rows, columns = queries.shape
    return pl.pallas_call(
        attend_kernel,
        grid=(count,),
        out_shape=jax.ShapeDtypeStruct((count, rows + extra, kv.shape[2]), jnp.bfloat16),
        in_specs=[SMEM, pl.BlockSpec((1, rows, columns), lambda i: (i, 0, 0)), VMEM],
        out_specs=pl.BlockSpec((1, rows + extra, kv.shape[2]), lambda i: (i, 0, 0)),
        name="attend",
    )(place, queries, kv)


def finish(lambdas, parts, gate, conv, head_gain, attn_w, conv_w):
    rows = gate.shape[0]
    return pl.pallas_call(
        finish_kernel,
        out_shape=(
            jax.ShapeDtypeStruct((rows, attn_w.shape[1]), jnp.bfloat16),
            jax.ShapeDtypeStruct((1, 2, rows), jnp.float32),
        ),
        in_specs=[SMEM] + [VMEM] * 6,
        out_specs=(VMEM, VMEM),
        name="finish",
    )(lambdas, parts, gate, conv, head_gain.reshape(1, -1), attn_w, conv_w)


def convolve(outer, insig, taps):
    rows = insig.shape[0]
    reach = taps.shape[0] - 1
    count = lax.axis_size("sp")
    before = lax.ppermute(insig[rows - reach :], "sp", [(i, i + 1) for i in range(count - 1)])
    extended = jnp.concatenate([before, insig], axis=0).astype(jnp.float32)
    summed = jnp.zeros(insig.shape, jnp.float32)
    for j in range(reach + 1):
        summed = summed + taps[j] * extended[j : j + rows]
    return (outer.astype(jnp.float32) * summed).astype(jnp.bfloat16)


def per_device(
    tokens,
    norm_gain,
    query_weight,
    key_weight,
    value_weight,
    gate_weight,
    outer_weight,
    inner_weight,
    signal_weight,
    conv_taps,
    lambdas,
    head_gain,
    attn_out_weight,
    conv_out_weight,
):
    chunk = 8
    tp = lax.axis_size("tp")
    sp = lax.axis_size("sp")
    near = [[g * chunk + i for i in range(chunk)] for g in range(sp // chunk)]
    far = [[g * chunk + i for g in range(sp // chunk)] for i in range(chunk)]
    same_core = [[2 * x + c for x in range(tp // 2)] for c in range(2)]
    core = lax.rem(lax.axis_index("tp"), 2)
    index = lax.axis_index("sp")

    own = lax.all_gather(tokens, "tp", axis_index_groups=same_core)
    other = lax.ppermute(own, "tp", [(i, i ^ 1) for i in range(tp)])
    kv, query, gate, outer, insig = project(
        core,
        own,
        other,
        norm_gain,
        (query_weight, key_weight, value_weight, gate_weight, outer_weight, inner_weight, signal_weight),
    )
    all_kv = lax.all_gather(kv, "sp", axis_index_groups=far)
    queries = lax.all_gather(query, "sp", axis_index_groups=near)
    conv = convolve(outer, insig, conv_taps)
    place = jnp.stack([lax.div(index, chunk), lax.rem(index, chunk)]).astype(jnp.int32)
    parts = attend(place, queries, all_kv, 16)
    parts = lax.all_to_all(parts, "sp", 0, 0, axis_index_groups=near, tiled=True)
    partial, log_totals = finish(lambdas, parts, gate, conv, head_gain, attn_out_weight, conv_out_weight)
    tiles = lax.all_to_all(partial.reshape(tp, -1, partial.shape[1]), "tp", 0, 0, tiled=True)
    mixed = jnp.sum(tiles.astype(jnp.float32), axis=0).astype(jnp.bfloat16)
    return mixed, log_totals


def solution(mesh):
    placed = (
        P("sp", "tp"),
        P(),
        P(None, "tp"),
        P(None, "tp"),
        P(None, "tp"),
        P(None, "tp"),
        P(None, "tp"),
        P(None, "tp"),
        P(None, "tp"),
        P(None, "tp"),
        P("tp"),
        P("tp"),
        P("tp", None),
        P("tp", None),
    )
    return jax.shard_map(
        per_device,
        mesh=mesh,
        in_specs=placed,
        out_specs=(P(("sp", "tp"), None), P("tp", None, "sp")),
        check_vma=False,
    )
```

time: 437 us -> 153 us (0.35)
  waiting for transfers between devices: 172 us -> 28.1 us
  matrix products: 87.5 us -> 0 us
  local copies, waits for them, and re-layouts: 87.7 us -> 1.82 us
  blocking collectives: 0 us -> 66.7 us
  loops' own time: 44.2 us -> 0 us
  Pallas kernels: 0 us -> 28.6 us
  other arithmetic: 14.7 us -> 2.18 us
    all_gather x1, waiting for transfers between devices: 144 us -> 19.5 us  [per_device(): all_kv = lax.all_gather(kv, 'sp', axis_index_groups=far)]
    dot_general x65 -> x0, matrix products: 87.5 us -> none  [the longest x31 42.9 us: absorb(): jnp.einsum('hmqk,khd->hmqd', weights_now.astype(jnp.bfloat16), value_bloc...]
    all_gather x0 -> x2, blocking collectives: none -> 46.4 us  [the longest x1 33 us: per_device(): queries = lax.all_gather(query, 'sp', axis_index_groups=near)]
    another operation x33 -> x0, loops' own time: 44.2 us -> none  [the longest x1 42.4 us: per_device(): lax.scan(one_block, carry, (key_blocks, value_blocks, jnp.arange(length /...]
    pallas_call x0 -> x3, Pallas kernels: none -> 28.6 us  [the longest x1 19.1 us: attend(): pl.pallas_call(attend_kernel, grid=(count,), out_shape=jax.ShapeDtypeStru...]
    all_to_all x2 -> x1, waiting for transfers between devices: 23.9 us -> 0.01 us  [per_device(): lax.all_to_all(parts, 'sp', 0, 0, axis_index_groups=near, tiled=True)]
    all_to_all x0 -> x1, blocking collectives: none -> 20.3 us  [per_device(): lax.all_to_all(partial.reshape(tp, -1, partial.shape[1]), 'tp', 0, 0, til...]
    slice x33 -> x1, local copies, waits for them, and re-layouts: 19.4 us -> 0.01 us  [convolve(): insig[rows - reach:]]
  transfers between devices with their start and end apart: 4 -> 4, of which waited for: 4 -> 3; matrix products, arithmetic and copies ran while one was open for 2% -> 1% of each run, Pallas kernels for 0% -> 0%
where the time goes in v1:
time: 153 us; the launch traced here: 152 us
  blocking collectives  66.7 us (44%)
  Pallas kernels  28.6 us (19%)
  waiting for transfers between devices  28.1 us (18%)
  between operations  14.7 us (10%)
  starting transfers between devices  10 us (7%)
  other arithmetic  2.18 us (1%)
  local copies, waits for them, and re-layouts  1.82 us (1%)
    all_gather x1, blocking collectives, per_device(): queries = lax.all_gather(query, 'sp', axis_index_groups=near)  33 us
    all_to_all x1, blocking collectives, per_device(): lax.all_to_all(partial.reshape(tp, -1, partial.shape[1]), 'tp', 0, 0, til...  20.3 us
    all_gather x1, waiting for transfers between devices, per_device(): all_kv = lax.all_gather(kv, 'sp', axis_index_groups=far)  19.5 us
    pallas_call x1, Pallas kernels, attend(): pl.pallas_call(attend_kernel, grid=(count,), out_shape=jax.ShapeDtypeStru...  19.1 us
    all_gather x1, blocking collectives, per_device(): own = lax.all_gather(tokens, 'tp', axis_index_groups=same_core)  13.3 us
    ppermute x1, waiting for transfers between devices, convolve(): lax.ppermute(insig[rows - reach:], 'sp', [(i, i + 1) for i in range(count...  6.68 us
    pallas_call x1, Pallas kernels, project(): pl.pallas_call(project_kernel, out_shape=(jax.ShapeDtypeStruct((rows, 2 *...  5.25 us
    all_to_all x1, starting transfers between devices, per_device(): lax.all_to_all(parts, 'sp', 0, 0, axis_index_groups=near, tiled=True)  4.71 us
  transfers between devices with their start and end apart: 4, of which 3 were waited for; matrix products, arithmetic and copies ran while one was open for 1% of the time, Pallas kernels for 0%

profile of v1, /device:TPU:480, one launch (start us, length us, event | category | flops | bytes accessed | tf_op | source)
XLA Modules:
  0.0 152.1 jit_solution(12146431271879313915)
XLA Ops:
  7.2 0.0 all-gather.5.cloned.1.call-start
  7.2 13.3 %all-gather = bf16[1024,256]{1,0:T(8,128)(2,1)S(1)} all-gather(bf16[256,256]{1,0:T(8,128)(2,1)} %param.14), channel_id=2, replica_groups={{0,2,4,6},{1,3,5,7},{8,10,12,14},{9,11,13,15},{16,18,20,22},{17,19,21,2..., dimensions={0}, use_global_device_ids=true | all-gather | bytes 655360 | tf_op jit(solution)/shard_map/all_gather | solution.py:223
  20.6 0.0 copy-start.1
  20.6 1.9 %collective-permute-start = (bf16[4,256,256]{2,1,0:T(8,128)(2,1)S(1)}, bf16[4,256,256]{2,1,0:T(8,128)(2,1)S(1)}, u32[]{:S(2)}, u32[]{:S(2)}) collective-permute-start(bf16[4,256,256]{2,1,0:T(8,128)(2,1)S(1)} %bitcast.15), channel_id=1, source_target_pairs={{0,1},{1,0},{2,3},{3,2},{4,5},{5,4},{6,7},{7,6},{8,9},{9,8},{10,11... | collective-permute-start | bytes 1572872 | tf_op jit(solution)/shard_map/ppermute | solution.py:224
  22.5 1.9 %collective-permute-done.other = bf16[4,256,256]{2,1,0:T(8,128)(2,1)S(1)} collective-permute-done((bf16[4,256,256]{2,1,0:T(8,128)(2,1)S(1)}, bf16[4,256,256]{2,1,0:T(8,128)(2,1)S(1)}, u32[]{:S(2)}, u32[]{:S(2)}) %collective-permute-start) | collective-permute-done | bytes 524320 | tf_op jit(solution)/shard_map/ppermute | solution.py:224
  24.4 0.0 copy-start.2
  24.4 0.0 copy-done.1
  24.4 0.8 copy-done.2
  25.1 5.3 %project.1 = (bf16[256,256]{1,0:T(8,128)(2,1)}, bf16[256,128]{1,0:T(8,128)(2,1)}, bf16[256,128]{1,0:T(8,128)(2,1)}, bf16[256,128]{1,0:T(8,128)(2,1)}, bf16[256,128]{1,0:T(8,128)(2,1)}) custom-call(s32[1]{0:T(128)} %bitcast.2.place, bf16[4,256,256]{2,1,0:T(8,128)(2,1)} %bitcast.16, bf16[4,256,256]{2,1,0:T(8,128)(2,1)} %copy-done.2, f32[1,2048]{1,0:T(1,128)} %bitcast.20, ...), custom_call_target="tpu_custom_call" | custom-call | tf_op jit(solution)/shard_map/project/pallas_call | solution.py:150
  30.4 0.0 all-gather.5.cloned.1.call-update
  30.4 0.7 pad_add_fusion.place
  31.1 33.0 %all-gather.1 = bf16[2048,128]{1,0:T(8,128)(2,1)} all-gather(bf16[256,128]{1,0:T(8,128)(2,1)} %get-tuple-element.9), channel_id=3, replica_groups={{0,8,16,24,32,40,48,56},{64,72,80,88,96,104,112,120},{128,136,144,152,1..., dimensions={0}, use_global_device_ids=true | all-gather | bytes 589824 | tf_op jit(solution)/shard_map/all_gather | solution.py:233
  64.1 19.5 %all-gather.5.cloned.1.call-done = bf16[2048,256]{1,0:T(8,128)(2,1)} async-done(((bf16[256,256]{1,0:T(8,128)(2,1)}), bf16[2048,256]{1,0:T(8,128)(2,1)}) %all-gather.5.cloned.1.call-update) | async-done | bytes 1048592 | tf_op jit(solution)/shard_map/all_gather | solution.py:232
  83.6 19.1 %attend.1 = bf16[8,272,256]{2,1,0:T(8,128)(2,1)} custom-call(s32[2]{0:T(128)} %pad_add_fusion.place, bf16[8,256,128]{2,1,0:T(8,128)(2,1)} %bitcast.17, bf16[8,256,256]{2,1,0:T(8,128)(2,1)} %bitcast.18), custom_call_target="tpu_custom_call" | custom-call | tf_op jit(solution)/shard_map/attend/pallas_call | solution.py:162
  102.7 0.0 copy-start.4
  102.7 0.0 copy-start.5
  102.7 0.0 copy-start.3
  102.7 4.7 %all-to-all-start = ((bf16[8,272,256]{2,1,0:T(8,128)(2,1)}), bf16[8,272,256]{2,1,0:T(8,128)(2,1)S(1)}, u32[]{:S(2)}, u32[]{:S(2)}) async-start(bf16[8,272,256]{2,1,0:T(8,128)(2,1)} %attend.1), calls=%async_computation | async-start | bytes 2228224 | tf_op jit(solution)/shard_map/all_to_all | solution.py:237
  107.4 0.0 copy-done.4
  107.4 3.4 %collective-permute-start.1 = (bf16[2,128]{1,0:T(2,128)(2,1)S(1)}, bf16[2,128]{1,0:T(2,128)(2,1)S(1)}, u32[]{:S(2)}, u32[]{:S(2)}) collective-permute-start(bf16[2,128]{1,0:T(2,128)(2,1)S(1)} %slice.22), channel_id=1, source_target_pairs={{0,8},{8,16},{16,24},{24,32},{32,40},{40,48},{48,56},{56,64},{64,7... | collective-permute-start | bytes 1544 | tf_op jit(solution)/shard_map/ppermute | solution.py:190
  110.8 0.0 copy-done.5
  111.4 6.7 %collective-permute-done.1 = bf16[2,128]{1,0:T(2,128)(2,1)S(1)} collective-permute-done((bf16[2,128]{1,0:T(2,128)(2,1)S(1)}, bf16[2,128]{1,0:T(2,128)(2,1)S(1)}, u32[]{:S(2)}, u32[]{:S(2)}) %collective-permute-start.1) | collective-permute-done | bytes 544 | tf_op jit(solution)/shard_map/ppermute | solution.py:190
  118.2 0.0 copy-done.3
  118.2 0.7 fusion.2.conv
  118.9 0.0 all-to-all-done.parts
  118.9 0.0 copy-start
  118.9 1.0 copy-done
  119.9 4.3 %finish.1 = (bf16[256,2048]{1,0:T(8,128)(2,1)}, f32[1,2,256]{2,1,0:T(2,128)}) custom-call(f32[1]{0:T(128)S(6)} %copy.16.lam, bf16[8,272,256]{2,1,0:T(8,128)(2,1)} %copy-done, bf16[256,128]{1,0:T(8,128)(2,1)} %get-tuple-element.11.gate, bf16[256,128]{1,0:T(8,128)(2,1)} %fusion.2.conv, f32[1,128]{1,0:T(1,128)} %bitcast.21, bf16[128,2048]{1,0:T(8,128)(2,1)} %attn_w.1, ...), custom_call_target="tpu_custom_call" | custom-call | tf_op jit(solution)/shard_map/finish/pallas_call | solution.py:174
  124.2 20.3 %all_to_all.10 = bf16[8,32,2048]{2,1,0:T(8,128)(2,1)S(1)} all-to-all(bf16[8,32,2048]{2,1,0:T(8,128)(2,1)} %bitcast.19), channel_id=1, replica_groups=mesh['sp'=64,'tp'=8] {'tp'}, dimensions={0} | all-to-all | bytes 2097152 | tf_op jit(solution)/shard_map/all_to_all | solution.py:239
  144.5 0.8 reduce_sum.12
  (3 shorter events, 0.0 us)
Async XLA Ops:
  7.2 76.4 %all-gather.5.cloned.1.call-start = ((), (), s32[]{:S(2)}) async-start(), calls=%async_computation.2 | async-start | bytes 1179648 | tf_op jit(solution)/shard_map/all_gather | solution.py:232
  20.6 3.8 %copy-start.1 = (bf16[1024,256]{1,0:T(8,128)(2,1)}, bf16[1024,256]{1,0:T(8,128)(2,1)S(1)}, u32[]{:S(2)}) copy-start(bf16[1024,256]{1,0:T(8,128)(2,1)S(1)} %all-gather) | copy-start | bytes 1572868
  20.6 3.8 %collective-permute-start = (bf16[4,256,256]{2,1,0:T(8,128)(2,1)S(1)}, bf16[4,256,256]{2,1,0:T(8,128)(2,1)S(1)}, u32[]{:S(2)}, u32[]{:S(2)}) collective-permute-start(bf16[4,256,256]{2,1,0:T(8,128)(2,1)S(1)} %bitcast.15), channel_id=1, source_target_pairs={{0,1},{1,0},{2,3},{3,2},{4,5},{5,4},{6,7},{7,6},{8,9},{9,8},{10,11... | collective-permute-start | bytes 1572872 | tf_op jit(solution)/shard_map/ppermute | solution.py:224
  24.4 0.8 copy-start.2
  102.7 4.7 %copy-start.4 = (bf16[256,128]{1,0:T(8,128)(2,1)S(1)}, bf16[256,128]{1,0:T(8,128)(2,1)}, u32[]{:S(2)}) copy-start(bf16[256,128]{1,0:T(8,128)(2,1)} %get-tuple-element.13) | copy-start | bytes 196612
  102.7 8.1 %copy-start.5 = (f32[3,128]{1,0:T(4,128)S(1)}, f32[3,128]{1,0:T(4,128)}, u32[]{:S(2)}) copy-start(f32[3,128]{1,0:T(4,128)} %param.23) | copy-start | bytes 4612
  102.7 15.5 %copy-start.3 = (bf16[256,128]{1,0:T(8,128)(2,1)S(1)}, bf16[256,128]{1,0:T(8,128)(2,1)}, u32[]{:S(2)}) copy-start(bf16[256,128]{1,0:T(8,128)(2,1)} %get-tuple-element.12) | copy-start | bytes 196612
  102.7 16.2 %all-to-all-start = ((bf16[8,272,256]{2,1,0:T(8,128)(2,1)}), bf16[8,272,256]{2,1,0:T(8,128)(2,1)S(1)}, u32[]{:S(2)}, u32[]{:S(2)}) async-start(bf16[8,272,256]{2,1,0:T(8,128)(2,1)} %attend.1), calls=%async_computation | async-start | bytes 2228224 | tf_op jit(solution)/shard_map/all_to_all | solution.py:237
  107.4 10.7 %collective-permute-start.1 = (bf16[2,128]{1,0:T(2,128)(2,1)S(1)}, bf16[2,128]{1,0:T(2,128)(2,1)S(1)}, u32[]{:S(2)}, u32[]{:S(2)}) collective-permute-start(bf16[2,128]{1,0:T(2,128)(2,1)S(1)} %slice.22), channel_id=1, source_target_pairs={{0,8},{8,16},{16,24},{24,32},{32,40},{40,48},{48,56},{56,64},{64,7... | collective-permute-start | bytes 1544 | tf_op jit(solution)/shard_map/ppermute | solution.py:190
  118.9 1.0 copy-start
Sparse Core Ops, SparseCore 0:
  30.5 53.0 all-gather.4

commit v2 on v1

--- a/solution.py
+++ b/solution.py
@@ -36,7 +36,9 @@
         columns = kw.shape[1]
         kv[:, :columns] = project(kw)
         kv[:, columns:] = project(vw)
-        q[...] = project(qw, LOG2E * (columns // 2) ** -0.5)
+        query = project(qw, LOG2E * (columns // 2) ** -0.5)
+        for i in range(q.shape[0]):
+            q[i] = query
         insig[...] = (project(iw).astype(jnp.float32) * project(sw).astype(jnp.float32)).astype(jnp.bfloat16)
         outer[...] = project(ow)
         gate[...] = project(gw)
@@ -45,42 +47,46 @@
         pl.when(place[0] == core)(functools.partial(spread, core))
 
 
-def attend_kernel(place, q, kv, out):
+def attend_kernel(place, q, *refs):
+    blocks, out = refs[:-1], refs[-1]
     rows = q.shape[1]
-    blocks, block_len, columns = kv.shape
+    columns = blocks[0].shape[1]
+    half = len(blocks) // 2
     value_size = columns // 2
     key_size = value_size // 2
-    step = pl.program_id(0)
     last = place[0]
     slot = place[1]
-    ahead = (step - slot) * rows
+    ahead = (pl.program_id(0) - slot) * rows
     queries = q[0]
-    ones = jnp.ones((block_len, value_size), jnp.bfloat16)
 
     def body(used):
+        chosen = blocks[1:used] if used <= half else blocks[1 : used + 1]
+        chosen = (*chosen, blocks[0])
         stats = []
         for m in range(2):
             query = queries[:, m * key_size : (m + 1) * key_size]
             scores = []
-            for b in range(used):
-                keys = kv[b][:, m * key_size : (m + 1) * key_size]
+            for ref in chosen:
+                keys = ref[:, m * key_size : (m + 1) * key_size]
                 scores.append(
                     lax.dot_general(query, keys, (((1,), (1,)), ((), ())), preferred_element_type=jnp.float32)
                 )
-            row = lax.broadcasted_iota(jnp.int32, (rows, block_len), 0)
-            col = lax.broadcasted_iota(jnp.int32, (rows, block_len), 1)
+            row = lax.broadcasted_iota(jnp.int32, (rows, rows), 0)
+            col = lax.broadcasted_iota(jnp.int32, (rows, rows), 1)
             seen = row + ahead >= col
             scores[-1] = jnp.where(seen, scores[-1], HIDDEN)
-            top = scores[0]
-            for s in scores[1:]:
+            tops = [s[:, i : i + value_size] for s in scores for i in range(0, s.shape[1], value_size)]
+            top = tops[0]
+            for s in tops[1:]:
                 top = jnp.maximum(top, s)
             top = jnp.max(top, axis=-1, keepdims=True)
             summed = jnp.zeros((rows, 2 * value_size), jnp.float32)
-            for b in range(used):
-                w = jnp.exp2(scores[b] - top)
-                if b == used - 1:
+            for ref, score in zip(chosen, scores):
+                w = jnp.exp2(score - top)
+                if ref is blocks[0]:
                     w = jnp.where(seen, w, 0.0)
-                values = jnp.concatenate([kv[b][:, value_size:], ones], axis=1)
+                ones = jnp.ones((ref.shape[0], value_size), jnp.bfloat16)
+                values = jnp.concatenate([ref[:, value_size:], ones], axis=1)
                 summed = summed + jnp.dot(w.astype(jnp.bfloat16), values, preferred_element_type=jnp.float32)
             total = summed[:, value_size:]
             some = total > 0.0
@@ -100,7 +106,7 @@
         turned = jnp.transpose(spread)
         out[0, rows:, :] = turned[: out.shape[1] - rows].astype(jnp.bfloat16)
 
-    for used in range(1, blocks + 1):
+    for used in range(1, len(blocks)):
         pl.when(last == used - 1)(functools.partial(body, used))
 
 
@@ -142,14 +148,20 @@
 SMEM = pl.BlockSpec(memory_space=pltpu.SMEM)
 
 
-def project(core, own, other, gain, weights):
+def project(core, own, other, gain, weights, copies):
     rows = own.shape[1]
     width = gain.shape[0]
     columns = weights[0].shape[1]
     narrow = jax.ShapeDtypeStruct((rows, columns), jnp.bfloat16)
     return pl.pallas_call(
         project_kernel,
-        out_shape=(jax.ShapeDtypeStruct((rows, 2 * columns), jnp.bfloat16), narrow, narrow, narrow, narrow),
+        out_shape=(
+            jax.ShapeDtypeStruct((rows, 2 * columns), jnp.bfloat16),
+            jax.ShapeDtypeStruct((copies, rows, columns), jnp.bfloat16),
+            narrow,
+            narrow,
+            narrow,
+        ),
         in_specs=[SMEM] + [VMEM] * 10,
         out_specs=(VMEM,) * 5,
         scratch_shapes=[pltpu.VMEM((rows, width), jnp.bfloat16)],
@@ -157,16 +169,17 @@
     )(core.reshape(1), own, other, gain.reshape(1, width), *weights)
 
 
-def attend(place, queries, kv, extra):
+def attend(place, queries, blocks, extra):
     count, rows, columns = queries.shape
+    wide = blocks[0].shape[1]
     return pl.pallas_call(
         attend_kernel,
         grid=(count,),
-        out_shape=jax.ShapeDtypeStruct((count, rows + extra, kv.shape[2]), jnp.bfloat16),
-        in_specs=[SMEM, pl.BlockSpec((1, rows, columns), lambda i: (i, 0, 0)), VMEM],
-        out_specs=pl.BlockSpec((1, rows + extra, kv.shape[2]), lambda i: (i, 0, 0)),
+        out_shape=jax.ShapeDtypeStruct((count, rows + extra, wide), jnp.bfloat16),
+        in_specs=[SMEM, pl.BlockSpec((1, rows, columns), lambda i: (i, 0, 0))] + [VMEM] * len(blocks),
+        out_specs=pl.BlockSpec((1, rows + extra, wide), lambda i: (i, 0, 0)),
         name="attend",
-    )(place, queries, kv)
+    )(place, queries, *blocks)
 
 
 def finish(lambdas, parts, gate, conv, head_gain, attn_w, conv_w):
@@ -181,6 +194,23 @@
         out_specs=(VMEM, VMEM),
         name="finish",
     )(lambdas, parts, gate, conv, head_gain.reshape(1, -1), attn_w, conv_w)
+
+
+def around(block, chunk):
+    devices = lax.axis_size("sp")
+    count = devices // chunk
+    half = block.shape[0] // 2
+
+    def moved(array, by):
+        return lax.ppermute(array, "sp", [(i, (i + by * chunk) % devices) for i in range(devices)])
+
+    ups, downs = [block], [block]
+    for _ in range(count // 2 - 1):
+        ups.append(moved(ups[-1], 1))
+        downs.append(moved(downs[-1], -1))
+    ups.append(moved(ups[-1][:half], 1))
+    downs.append(moved(downs[-1][half:], -1))
+    return ups + downs[:0:-1]
 
 
 def convolve(outer, insig, taps):
@@ -215,7 +245,6 @@
     tp = lax.axis_size("tp")
     sp = lax.axis_size("sp")
     near = [[g * chunk + i for i in range(chunk)] for g in range(sp // chunk)]
-    far = [[g * chunk + i for g in range(sp // chunk)] for i in range(chunk)]
     same_core = [[2 * x + c for x in range(tp // 2)] for c in range(2)]
     core = lax.rem(lax.axis_index("tp"), 2)
     index = lax.axis_index("sp")
@@ -228,12 +257,13 @@
         other,
         norm_gain,
         (query_weight, key_weight, value_weight, gate_weight, outer_weight, inner_weight, signal_weight),
+        chunk,
     )
-    all_kv = lax.all_gather(kv, "sp", axis_index_groups=far)
-    queries = lax.all_gather(query, "sp", axis_index_groups=near)
+    queries = lax.all_to_all(query, "sp", 0, 0, axis_index_groups=near, tiled=True)
+    blocks = around(kv, chunk)
     conv = convolve(outer, insig, conv_taps)
     place = jnp.stack([lax.div(index, chunk), lax.rem(index, chunk)]).astype(jnp.int32)
-    parts = attend(place, queries, all_kv, 16)
+    parts = attend(place, queries, blocks, 16)
     parts = lax.all_to_all(parts, "sp", 0, 0, axis_index_groups=near, tiled=True)
     partial, log_totals = finish(lambdas, parts, gate, conv, head_gain, attn_out_weight, conv_out_weight)
     tiles = lax.all_to_all(partial.reshape(tp, -1, partial.shape[1]), "tp", 0, 0, tiled=True)

time: 153 us -> 142 us (0.928)
  starting transfers between devices: 10 us -> 46.7 us
  blocking collectives: 66.7 us -> 33.3 us
  between operations: 14.7 us -> 1.52 us
  waiting for transfers between devices: 28.1 us -> 23.5 us
  Pallas kernels: 28.6 us -> 30.3 us
    all_gather x1 -> x0, blocking collectives: 33 us -> none  [per_device(): queries = lax.all_gather(query, 'sp', axis_index_groups=near)]
    ppermute x0 -> x8, starting transfers between devices: none -> 28.7 us  [moved(): lax.ppermute(array, 'sp', [(i, (i + by * chunk) % devices) for i in range...]
    all_gather x1 -> x0, waiting for transfers between devices: 19.5 us -> none  [per_device(): all_kv = lax.all_gather(kv, 'sp', axis_index_groups=far)]
    ppermute x0 -> x8, waiting for transfers between devices: none -> 13.7 us  [moved(): lax.ppermute(array, 'sp', [(i, (i + by * chunk) % devices) for i in range...]
    all_to_all x0 -> x1, starting transfers between devices: none -> 5.94 us  [per_device(): lax.all_to_all(query, 'sp', 0, 0, axis_index_groups=near, tiled=True)]
    all_to_all x1, starting transfers between devices: 4.71 us -> 6.78 us  [per_device(): lax.all_to_all(parts, 'sp', 0, 0, axis_index_groups=near, tiled=True)]
    pallas_call x1, Pallas kernels: 19.1 us -> 20.7 us  [attend(): pl.pallas_call(attend_kernel, grid=(count,), out_shape=jax.ShapeDtypeStru...]
    unnamed x12 -> x30, local copies, waits for them, and re-layouts: 1.81 us -> 3.2 us
  transfers between devices with their start and end apart: 4 -> 12, of which waited for: 3 -> 7; matrix products, arithmetic and copies ran while one was open for 1% -> 1% of each run, Pallas kernels for 0% -> 0%
where the time goes in v2:
time: 142 us; the launch traced here: 141 us
  starting transfers between devices  46.7 us (33%)
  blocking collectives  33.3 us (23%)
  Pallas kernels  30.3 us (21%)
  waiting for transfers between devices  23.5 us (17%)
  local copies, waits for them, and re-layouts  3.23 us (2%)
  other arithmetic  2.18 us (2%)
  between operations  1.52 us (1%)
    ppermute x8, starting transfers between devices, moved(): lax.ppermute(array, 'sp', [(i, (i + by * chunk) % devices) for i in range...  28.7 us
    pallas_call x1, Pallas kernels, attend(): pl.pallas_call(attend_kernel, grid=(count,), out_shape=jax.ShapeDtypeStru...  20.7 us
    all_to_all x1, blocking collectives, per_device(): lax.all_to_all(partial.reshape(tp, -1, partial.shape[1]), 'tp', 0, 0, til...  19.9 us
    ppermute x8, waiting for transfers between devices, moved(): lax.ppermute(array, 'sp', [(i, (i + by * chunk) % devices) for i in range...  13.7 us
    all_gather x1, blocking collectives, per_device(): own = lax.all_gather(tokens, 'tp', axis_index_groups=same_core)  13.3 us
    ppermute x1, waiting for transfers between devices, convolve(): lax.ppermute(insig[rows - reach:], 'sp', [(i, i + 1) for i in range(count...  7.94 us
    all_to_all x1, starting transfers between devices, per_device(): lax.all_to_all(parts, 'sp', 0, 0, axis_index_groups=near, tiled=True)  6.78 us
    all_to_all x1, starting transfers between devices, per_device(): lax.all_to_all(query, 'sp', 0, 0, axis_index_groups=near, tiled=True)  5.94 us
  transfers between devices with their start and end apart: 12, of which 7 were waited for; matrix products, arithmetic and copies ran while one was open for 1% of the time, Pallas kernels for 0%

profile of v2, /device:TPU:480, one launch (start us, length us, event | category | flops | bytes accessed | tf_op | source)
XLA Modules:
  0.0 140.8 jit_solution(4446312440149582728)
XLA Ops:
  0.6 13.3 %all-gather = bf16[1024,256]{1,0:T(8,128)(2,1)S(1)} all-gather(bf16[256,256]{1,0:T(8,128)(2,1)} %param.14), channel_id=2, replica_groups={{0,2,4,6},{1,3,5,7},{8,10,12,14},{9,11,13,15},{16,18,20,22},{17,19,21,2..., dimensions={0}, use_global_device_ids=true | all-gather | bytes 655360 | tf_op jit(solution)/shard_map/all_gather | solution.py:252
  14.0 1.9 %collective-permute-start = (bf16[4,256,256]{2,1,0:T(8,128)(2,1)S(1)}, bf16[4,256,256]{2,1,0:T(8,128)(2,1)S(1)}, u32[]{:S(2)}, u32[]{:S(2)}) collective-permute-start(bf16[4,256,256]{2,1,0:T(8,128)(2,1)S(1)} %bitcast.13), channel_id=1, source_target_pairs={{0,1},{1,0},{2,3},{3,2},{4,5},{5,4},{6,7},{7,6},{8,9},{9,8},{10,11... | collective-permute-start | bytes 1572872 | tf_op jit(solution)/shard_map/ppermute | solution.py:253
  15.9 1.9 %collective-permute-done.other = bf16[4,256,256]{2,1,0:T(8,128)(2,1)S(1)} collective-permute-done((bf16[4,256,256]{2,1,0:T(8,128)(2,1)S(1)}, bf16[4,256,256]{2,1,0:T(8,128)(2,1)S(1)}, u32[]{:S(2)}, u32[]{:S(2)}) %collective-permute-start) | collective-permute-done | bytes 524320 | tf_op jit(solution)/shard_map/ppermute | solution.py:253
  17.8 0.8 copy-done.3
  18.6 5.4 %project.1 = (bf16[256,256]{1,0:T(8,128)(2,1)}, bf16[8,256,128]{2,1,0:T(8,128)(2,1)}, bf16[256,128]{1,0:T(8,128)(2,1)}, bf16[256,128]{1,0:T(8,128)(2,1)}, bf16[256,128]{1,0:T(8,128)(2,1)}) custom-call(s32[1]{0:T(128)} %bitcast.2.place, bf16[4,256,256]{2,1,0:T(8,128)(2,1)} %bitcast.14, bf16[4,256,256]{2,1,0:T(8,128)(2,1)} %copy-done.3, f32[1,2048]{1,0:T(1,128)} %bitcast.16, ...), custom_call_target="tpu_custom_call" | custom-call | tf_op jit(solution)/shard_map/project/pallas_call | solution.py:156
  24.0 5.9 %all-to-all-start = ((bf16[8,256,128]{2,1,0:T(8,128)(2,1)}), bf16[8,256,128]{2,1,0:T(8,128)(2,1)S(1)}, u32[]{:S(2)}, u32[]{:S(2)}) async-start(bf16[8,256,128]{2,1,0:T(8,128)(2,1)} %get-tuple-element.9), calls=%async_computation | async-start | bytes 1048576 | tf_op jit(solution)/shard_map/all_to_all | solution.py:262
  29.9 1.9 %collective-permute-start.1 = (bf16[256,256]{1,0:T(8,128)(2,1)}, bf16[256,256]{1,0:T(8,128)(2,1)S(1)}, u32[]{:S(2)}, u32[]{:S(2)}) collective-permute-start(bf16[256,256]{1,0:T(8,128)(2,1)} %get-tuple-element.10.refs_0_), channel_id=1, source_target_pairs={{0,64},{8,72},{16,80},{24,88},{32,96},{40,104},{48,112},{56,120},{... | collective-permute-start | bytes 393224 | tf_op jit(solution)/shard_map/ppermute | solution.py:205
  31.8 4.8 %collective-permute-start.5 = (bf16[256,256]{1,0:T(8,128)(2,1)}, bf16[256,256]{1,0:T(8,128)(2,1)S(1)}, u32[]{:S(2)}, u32[]{:S(2)}) collective-permute-start(bf16[256,256]{1,0:T(8,128)(2,1)} %get-tuple-element.10.refs_0_), channel_id=1, source_target_pairs={{0,448},{8,456},{16,464},{24,472},{32,480},{40,488},{48,496},{56,5... | collective-permute-start | bytes 393224 | tf_op jit(solution)/shard_map/ppermute | solution.py:205
  36.7 1.7 %collective-permute-done.1.refs_1_ = bf16[256,256]{1,0:T(8,128)(2,1)S(1)} collective-permute-done((bf16[256,256]{1,0:T(8,128)(2,1)}, bf16[256,256]{1,0:T(8,128)(2,1)S(1)}, u32[]{:S(2)}, u32[]{:S(2)}) %collective-permute-start.1) | collective-permute-done | bytes 131104 | tf_op jit(solution)/shard_map/ppermute | solution.py:205
  38.3 3.1 %collective-permute-start.2 = (bf16[256,256]{1,0:T(8,128)(2,1)S(1)}, bf16[256,256]{1,0:T(8,128)(2,1)S(1)}, u32[]{:S(2)}, u32[]{:S(2)}) collective-permute-start(bf16[256,256]{1,0:T(8,128)(2,1)S(1)} %collective-permute-done.1.refs_1_), channel_id=1, source_target_pairs={{0,64},{8,72},{16,80},{24,88},{32,96},{40,104},{48,112},{56,120},{... | collective-permute-start | bytes 393224 | tf_op jit(solution)/shard_map/ppermute | solution.py:205
  41.4 1.2 collective-permute-done.5.refs_8_
  42.6 4.3 %collective-permute-start.6 = (bf16[256,256]{1,0:T(8,128)(2,1)S(1)}, bf16[256,256]{1,0:T(8,128)(2,1)S(1)}, u32[]{:S(2)}, u32[]{:S(2)}) collective-permute-start(bf16[256,256]{1,0:T(8,128)(2,1)S(1)} %collective-permute-done.5.refs_8_), channel_id=1, source_target_pairs={{0,448},{8,456},{16,464},{24,472},{32,480},{40,488},{48,496},{56,5... | collective-permute-start | bytes 393224 | tf_op jit(solution)/shard_map/ppermute | solution.py:205
  46.8 0.0 collective-permute-done.2.refs_2_
  46.8 3.7 %collective-permute-start.3 = (bf16[256,256]{1,0:T(8,128)(2,1)S(1)}, bf16[256,256]{1,0:T(8,128)(2,1)S(1)}, u32[]{:S(2)}, u32[]{:S(2)}) collective-permute-start(bf16[256,256]{1,0:T(8,128)(2,1)S(1)} %collective-permute-done.2.refs_2_), channel_id=1, source_target_pairs={{0,64},{8,72},{16,80},{24,88},{32,96},{40,104},{48,112},{56,120},{... | collective-permute-start | bytes 393224 | tf_op jit(solution)/shard_map/ppermute | solution.py:205
  50.5 3.4 %collective-permute-done.6.refs_7_ = bf16[256,256]{1,0:T(8,128)(2,1)S(1)} collective-permute-done((bf16[256,256]{1,0:T(8,128)(2,1)S(1)}, bf16[256,256]{1,0:T(8,128)(2,1)S(1)}, u32[]{:S(2)}, u32[]{:S(2)}) %collective-permute-start.6) | collective-permute-done | bytes 131104 | tf_op jit(solution)/shard_map/ppermute | solution.py:205
  53.9 3.0 %collective-permute-start.7 = (bf16[256,256]{1,0:T(8,128)(2,1)S(1)}, bf16[256,256]{1,0:T(8,128)(2,1)S(1)}, u32[]{:S(2)}, u32[]{:S(2)}) collective-permute-start(bf16[256,256]{1,0:T(8,128)(2,1)S(1)} %collective-permute-done.6.refs_7_), channel_id=1, source_target_pairs={{0,448},{8,456},{16,464},{24,472},{32,480},{40,488},{48,496},{56,5... | collective-permute-start | bytes 393224 | tf_op jit(solution)/shard_map/ppermute | solution.py:205
  56.9 5.0 %collective-permute-start.4 = (bf16[128,256]{1,0:T(8,128)(2,1)S(1)}, bf16[128,256]{1,0:T(8,128)(2,1)S(1)}, u32[]{:S(2)}, u32[]{:S(2)}) collective-permute-start(bf16[128,256]{1,0:T(8,128)(2,1)S(1)} %slice.36), channel_id=1, source_target_pairs={{0,64},{8,72},{16,80},{24,88},{32,96},{40,104},{48,112},{56,120},{... | collective-permute-start | bytes 196616 | tf_op jit(solution)/shard_map/ppermute | solution.py:205
  61.9 2.5 %collective-permute-done.7.refs_6_ = bf16[256,256]{1,0:T(8,128)(2,1)S(1)} collective-permute-done((bf16[256,256]{1,0:T(8,128)(2,1)S(1)}, bf16[256,256]{1,0:T(8,128)(2,1)S(1)}, u32[]{:S(2)}, u32[]{:S(2)}) %collective-permute-start.7) | collective-permute-done | bytes 131104 | tf_op jit(solution)/shard_map/ppermute | solution.py:205
  64.4 3.0 %collective-permute-start.8 = (bf16[128,256]{1,0:T(8,128)(2,1)S(1)}, bf16[128,256]{1,0:T(8,128)(2,1)S(1)}, u32[]{:S(2)}, u32[]{:S(2)}) collective-permute-start(bf16[128,256]{1,0:T(8,128)(2,1)S(1)} %slice.37), channel_id=1, source_target_pairs={{0,448},{8,456},{16,464},{24,472},{32,480},{40,488},{48,496},{56,5... | collective-permute-start | bytes 196616 | tf_op jit(solution)/shard_map/ppermute | solution.py:205
  67.4 0.7 pad_add_fusion.place
  68.1 5.1 %collective-permute-done.8.refs_5_ = bf16[128,256]{1,0:T(8,128)(2,1)S(1)} collective-permute-done((bf16[128,256]{1,0:T(8,128)(2,1)S(1)}, bf16[128,256]{1,0:T(8,128)(2,1)S(1)}, u32[]{:S(2)}, u32[]{:S(2)}) %collective-permute-start.8) | collective-permute-done | bytes 65568 | tf_op jit(solution)/shard_map/ppermute | solution.py:205
  73.2 0.5 copy-done.13
  73.8 0.8 copy-done.2
  74.6 20.7 %attend.1 = bf16[8,272,256]{2,1,0:T(8,128)(2,1)} custom-call(s32[2]{0:T(128)} %pad_add_fusion.place, bf16[8,256,128]{2,1,0:T(8,128)(2,1)} %copy-done.2, bf16[256,256]{1,0:T(8,128)(2,1)} %get-tuple-element.10.refs_0_, bf16[256,256]{1,0:T(8,128)(2,1)} %copy-done.6, bf16[256,256]{1,0:T(8,128)(2,1)} %copy-done.8, bf16[256,256]{1,0:T(8,128)(2,1)} %copy-done.4, ...), custom_call_target="tpu_custom_call" | custom-call | tf_op jit(solution)/shard_map/attend/pallas_call | solution.py:175
  95.3 6.8 %all-to-all-start.1 = ((bf16[8,272,256]{2,1,0:T(8,128)(2,1)}), bf16[8,272,256]{2,1,0:T(8,128)(2,1)S(1)}, u32[]{:S(2)}, u32[]{:S(2)}) async-start(bf16[8,272,256]{2,1,0:T(8,128)(2,1)} %attend.1), calls=%async_computation.1 | async-start | bytes 2228224 | tf_op jit(solution)/shard_map/all_to_all | solution.py:267
  102.0 3.4 %collective-permute-start.9 = (bf16[2,128]{1,0:T(2,128)(2,1)S(1)}, bf16[2,128]{1,0:T(2,128)(2,1)S(1)}, u32[]{:S(2)}, u32[]{:S(2)}) collective-permute-start(bf16[2,128]{1,0:T(2,128)(2,1)S(1)} %slice.30), channel_id=1, source_target_pairs={{0,8},{8,16},{16,24},{24,32},{32,40},{40,48},{48,56},{56,64},{64,7... | collective-permute-start | bytes 1544 | tf_op jit(solution)/shard_map/ppermute | solution.py:220
  106.1 7.9 %collective-permute-done.9 = bf16[2,128]{1,0:T(2,128)(2,1)S(1)} collective-permute-done((bf16[2,128]{1,0:T(2,128)(2,1)S(1)}, bf16[2,128]{1,0:T(2,128)(2,1)S(1)}, u32[]{:S(2)}, u32[]{:S(2)}) %collective-permute-start.9) | collective-permute-done | bytes 544 | tf_op jit(solution)/shard_map/ppermute | solution.py:220
  114.1 0.7 fusion.2.conv
  114.7 1.0 copy-done
  115.8 4.3 %finish.1 = (bf16[256,2048]{1,0:T(8,128)(2,1)}, f32[1,2,256]{2,1,0:T(2,128)}) custom-call(f32[1]{0:T(128)S(6)} %copy.16.lam, bf16[8,272,256]{2,1,0:T(8,128)(2,1)} %copy-done, bf16[256,128]{1,0:T(8,128)(2,1)} %get-tuple-element.11.gate, bf16[256,128]{1,0:T(8,128)(2,1)} %fusion.2.conv, f32[1,128]{1,0:T(1,128)} %bitcast.17, bf16[128,2048]{1,0:T(8,128)(2,1)} %attn_w.1, ...), custom_call_target="tpu_custom_call" | custom-call | tf_op jit(solution)/shard_map/finish/pallas_call | solution.py:187
  120.0 19.9 %all_to_all.15 = bf16[8,32,2048]{2,1,0:T(8,128)(2,1)S(1)} all-to-all(bf16[8,32,2048]{2,1,0:T(8,128)(2,1)} %bitcast.15), channel_id=1, replica_groups=mesh['sp'=64,'tp'=8] {'tp'}, dimensions={0} | all-to-all | bytes 2097152 | tf_op jit(solution)/shard_map/all_to_all | solution.py:269
  140.0 0.8 reduce_sum.12
  (35 shorter events, 0.1 us)
Async XLA Ops:
  14.0 3.8 %copy-start.1 = (bf16[1024,256]{1,0:T(8,128)(2,1)}, bf16[1024,256]{1,0:T(8,128)(2,1)S(1)}, u32[]{:S(2)}) copy-start(bf16[1024,256]{1,0:T(8,128)(2,1)S(1)} %all-gather) | copy-start | bytes 1572868
  14.0 3.8 %collective-permute-start = (bf16[4,256,256]{2,1,0:T(8,128)(2,1)S(1)}, bf16[4,256,256]{2,1,0:T(8,128)(2,1)S(1)}, u32[]{:S(2)}, u32[]{:S(2)}) collective-permute-start(bf16[4,256,256]{2,1,0:T(8,128)(2,1)S(1)} %bitcast.13), channel_id=1, source_target_pairs={{0,1},{1,0},{2,3},{3,2},{4,5},{5,4},{6,7},{7,6},{8,9},{9,8},{10,11... | collective-permute-start | bytes 1572872 | tf_op jit(solution)/shard_map/ppermute | solution.py:253
  17.8 0.8 copy-start.3
  24.0 49.2 %all-to-all-start = ((bf16[8,256,128]{2,1,0:T(8,128)(2,1)}), bf16[8,256,128]{2,1,0:T(8,128)(2,1)S(1)}, u32[]{:S(2)}, u32[]{:S(2)}) async-start(bf16[8,256,128]{2,1,0:T(8,128)(2,1)} %get-tuple-element.9), calls=%async_computation | async-start | bytes 1048576 | tf_op jit(solution)/shard_map/all_to_all | solution.py:262
  29.9 8.4 %collective-permute-start.1 = (bf16[256,256]{1,0:T(8,128)(2,1)}, bf16[256,256]{1,0:T(8,128)(2,1)S(1)}, u32[]{:S(2)}, u32[]{:S(2)}) collective-permute-start(bf16[256,256]{1,0:T(8,128)(2,1)} %get-tuple-element.10.refs_0_), channel_id=1, source_target_pairs={{0,64},{8,72},{16,80},{24,88},{32,96},{40,104},{48,112},{56,120},{... | collective-permute-start | bytes 393224 | tf_op jit(solution)/shard_map/ppermute | solution.py:205
  31.8 10.7 %collective-permute-start.5 = (bf16[256,256]{1,0:T(8,128)(2,1)}, bf16[256,256]{1,0:T(8,128)(2,1)S(1)}, u32[]{:S(2)}, u32[]{:S(2)}) collective-permute-start(bf16[256,256]{1,0:T(8,128)(2,1)} %get-tuple-element.10.refs_0_), channel_id=1, source_target_pairs={{0,448},{8,456},{16,464},{24,472},{32,480},{40,488},{48,496},{56,5... | collective-permute-start | bytes 393224 | tf_op jit(solution)/shard_map/ppermute | solution.py:205
  38.3 34.8 %copy-start.6 = (bf16[256,256]{1,0:T(8,128)(2,1)}, bf16[256,256]{1,0:T(8,128)(2,1)S(1)}, u32[]{:S(2)}) copy-start(bf16[256,256]{1,0:T(8,128)(2,1)S(1)} %collective-permute-done.1.refs_1_) | copy-start | bytes 393220
  38.3 8.5 %collective-permute-start.2 = (bf16[256,256]{1,0:T(8,128)(2,1)S(1)}, bf16[256,256]{1,0:T(8,128)(2,1)S(1)}, u32[]{:S(2)}, u32[]{:S(2)}) collective-permute-start(bf16[256,256]{1,0:T(8,128)(2,1)S(1)} %collective-permute-done.1.refs_1_), channel_id=1, source_target_pairs={{0,64},{8,72},{16,80},{24,88},{32,96},{40,104},{48,112},{56,120},{... | collective-permute-start | bytes 393224 | tf_op jit(solution)/shard_map/ppermute | solution.py:205
  42.6 30.6 %copy-start.7 = (bf16[256,256]{1,0:T(8,128)(2,1)}, bf16[256,256]{1,0:T(8,128)(2,1)S(1)}, u32[]{:S(2)}) copy-start(bf16[256,256]{1,0:T(8,128)(2,1)S(1)} %collective-permute-done.5.refs_8_) | copy-start | bytes 393220
  42.6 11.3 %collective-permute-start.6 = (bf16[256,256]{1,0:T(8,128)(2,1)S(1)}, bf16[256,256]{1,0:T(8,128)(2,1)S(1)}, u32[]{:S(2)}, u32[]{:S(2)}) collective-permute-start(bf16[256,256]{1,0:T(8,128)(2,1)S(1)} %collective-permute-done.5.refs_8_), channel_id=1, source_target_pairs={{0,448},{8,456},{16,464},{24,472},{32,480},{40,488},{48,496},{56,5... | collective-permute-start | bytes 393224 | tf_op jit(solution)/shard_map/ppermute | solution.py:205
  46.8 26.3 %copy-start.8 = (bf16[256,256]{1,0:T(8,128)(2,1)}, bf16[256,256]{1,0:T(8,128)(2,1)S(1)}, u32[]{:S(2)}) copy-start(bf16[256,256]{1,0:T(8,128)(2,1)S(1)} %collective-permute-done.2.refs_2_) | copy-start | bytes 393220
  46.8 10.0 %collective-permute-start.3 = (bf16[256,256]{1,0:T(8,128)(2,1)S(1)}, bf16[256,256]{1,0:T(8,128)(2,1)S(1)}, u32[]{:S(2)}, u32[]{:S(2)}) collective-permute-start(bf16[256,256]{1,0:T(8,128)(2,1)S(1)} %collective-permute-done.2.refs_2_), channel_id=1, source_target_pairs={{0,64},{8,72},{16,80},{24,88},{32,96},{40,104},{48,112},{56,120},{... | collective-permute-start | bytes 393224 | tf_op jit(solution)/shard_map/ppermute | solution.py:205
  53.9 19.3 %copy-start.9 = (bf16[256,256]{1,0:T(8,128)(2,1)}, bf16[256,256]{1,0:T(8,128)(2,1)S(1)}, u32[]{:S(2)}) copy-start(bf16[256,256]{1,0:T(8,128)(2,1)S(1)} %collective-permute-done.6.refs_7_) | copy-start | bytes 393220
  53.9 10.5 %collective-permute-start.7 = (bf16[256,256]{1,0:T(8,128)(2,1)S(1)}, bf16[256,256]{1,0:T(8,128)(2,1)S(1)}, u32[]{:S(2)}, u32[]{:S(2)}) collective-permute-start(bf16[256,256]{1,0:T(8,128)(2,1)S(1)} %collective-permute-done.6.refs_7_), channel_id=1, source_target_pairs={{0,448},{8,456},{16,464},{24,472},{32,480},{40,488},{48,496},{56,5... | collective-permute-start | bytes 393224 | tf_op jit(solution)/shard_map/ppermute | solution.py:205
  56.9 16.3 %copy-start.4 = (bf16[256,256]{1,0:T(8,128)(2,1)}, bf16[256,256]{1,0:T(8,128)(2,1)S(1)}, u32[]{:S(2)}) copy-start(bf16[256,256]{1,0:T(8,128)(2,1)S(1)} %collective-permute-done.3.refs_3_) | copy-start | bytes 393220
  56.9 11.2 %collective-permute-start.4 = (bf16[128,256]{1,0:T(8,128)(2,1)S(1)}, bf16[128,256]{1,0:T(8,128)(2,1)S(1)}, u32[]{:S(2)}, u32[]{:S(2)}) collective-permute-start(bf16[128,256]{1,0:T(8,128)(2,1)S(1)} %slice.36), channel_id=1, source_target_pairs={{0,64},{8,72},{16,80},{24,88},{32,96},{40,104},{48,112},{56,120},{... | collective-permute-start | bytes 196616 | tf_op jit(solution)/shard_map/ppermute | solution.py:205
  64.4 8.8 %copy-start.5 = (bf16[256,256]{1,0:T(8,128)(2,1)}, bf16[256,256]{1,0:T(8,128)(2,1)S(1)}, u32[]{:S(2)}) copy-start(bf16[256,256]{1,0:T(8,128)(2,1)S(1)} %collective-permute-done.7.refs_6_) | copy-start | bytes 393220
  64.4 8.8 %collective-permute-start.8 = (bf16[128,256]{1,0:T(8,128)(2,1)S(1)}, bf16[128,256]{1,0:T(8,128)(2,1)S(1)}, u32[]{:S(2)}, u32[]{:S(2)}) collective-permute-start(bf16[128,256]{1,0:T(8,128)(2,1)S(1)} %slice.37), channel_id=1, source_target_pairs={{0,448},{8,456},{16,464},{24,472},{32,480},{40,488},{48,496},{56,5... | collective-permute-start | bytes 196616 | tf_op jit(solution)/shard_map/ppermute | solution.py:205
  68.1 5.1 %copy-start.12 = (bf16[128,256]{1,0:T(8,128)(2,1)}, bf16[128,256]{1,0:T(8,128)(2,1)S(1)}, u32[]{:S(2)}) copy-start(bf16[128,256]{1,0:T(8,128)(2,1)S(1)} %collective-permute-done.4.refs_4_) | copy-start | bytes 196612
  73.1 0.6 copy-start.13
  73.8 0.8 copy-start.2
  95.2 6.8 %copy-start.11 = (bf16[256,128]{1,0:T(8,128)(2,1)S(1)}, bf16[256,128]{1,0:T(8,128)(2,1)}, u32[]{:S(2)}) copy-start(bf16[256,128]{1,0:T(8,128)(2,1)} %get-tuple-element.13) | copy-start | bytes 196612
  95.2 10.2 %copy-start.14 = (f32[3,128]{1,0:T(4,128)S(1)}, f32[3,128]{1,0:T(4,128)}, u32[]{:S(2)}) copy-start(f32[3,128]{1,0:T(4,128)} %param.23) | copy-start | bytes 4612
  95.2 18.8 %copy-start.10 = (bf16[256,128]{1,0:T(8,128)(2,1)S(1)}, bf16[256,128]{1,0:T(8,128)(2,1)}, u32[]{:S(2)}) copy-start(bf16[256,128]{1,0:T(8,128)(2,1)} %get-tuple-element.12) | copy-start | bytes 196612
  95.3 19.5 %all-to-all-start.1 = ((bf16[8,272,256]{2,1,0:T(8,128)(2,1)}), bf16[8,272,256]{2,1,0:T(8,128)(2,1)S(1)}, u32[]{:S(2)}, u32[]{:S(2)}) async-start(bf16[8,272,256]{2,1,0:T(8,128)(2,1)} %attend.1), calls=%async_computation.1 | async-start | bytes 2228224 | tf_op jit(solution)/shard_map/all_to_all | solution.py:267
  102.0 12.0 %collective-permute-start.9 = (bf16[2,128]{1,0:T(2,128)(2,1)S(1)}, bf16[2,128]{1,0:T(2,128)(2,1)S(1)}, u32[]{:S(2)}, u32[]{:S(2)}) collective-permute-start(bf16[2,128]{1,0:T(2,128)(2,1)S(1)} %slice.30), channel_id=1, source_target_pairs={{0,8},{8,16},{16,24},{24,32},{32,40},{40,48},{48,56},{56,64},{64,7... | collective-permute-start | bytes 1544 | tf_op jit(solution)/shard_map/ppermute | solution.py:220
  114.7 1.0 copy-start

commit v3 on v2

--- a/solution.py
+++ b/solution.py
@@ -12,7 +12,7 @@
 HIDDEN = -1e30
 
 
-def project_kernel(place, own, other, gain, qw, kw, vw, gw, ow, iw, sw, kv, q, gate, outer, insig, normed):
+def project_kernel(own, other, gain, qw, kw, vw, gw, ow, iw, sw, kv, q, gate, outer, insig, normed):
     count, rows, part = own.shape
     width = normed.shape[1]
 
@@ -44,70 +44,88 @@
         gate[...] = project(gw)
 
     for core in range(2):
-        pl.when(place[0] == core)(functools.partial(spread, core))
-
-
-def attend_kernel(place, q, *refs):
-    blocks, out = refs[:-1], refs[-1]
+        pl.when(lax.rem(lax.axis_index("tp"), 2) == core)(functools.partial(spread, core))
+
+
+def attend_kernel(chunk, span, q, own, kv, out, held):
     rows = q.shape[1]
-    columns = blocks[0].shape[1]
-    half = len(blocks) // 2
+    columns = kv.shape[2]
     value_size = columns // 2
     key_size = value_size // 2
-    last = place[0]
-    slot = place[1]
-    ahead = (pl.program_id(0) - slot) * rows
-    queries = q[0]
-
-    def body(used):
-        chosen = blocks[1:used] if used <= half else blocks[1 : used + 1]
-        chosen = (*chosen, blocks[0])
+    index = lax.axis_index("sp")
+    last = lax.div(index, chunk)
+    slot = lax.rem(index, chunk)
+    first = pl.program_id(0) * span
+    lane = lax.broadcasted_iota(jnp.int32, (rows, value_size), 1)
+    units = [(i, m) for i in range(span) for m in range(2)]
+
+    def body(full):
+        order = [*range(full), None]
+        ones = jnp.ones((rows, value_size), jnp.bfloat16)
+        row = lax.broadcasted_iota(jnp.int32, (rows, rows), 0)
+        col = lax.broadcasted_iota(jnp.int32, (rows, rows), 1)
+
+        def part(b, cut):
+            return own[:, cut] if b is None else kv[b, :, cut]
+
+        def seen(i):
+            return row + (first + i - slot) * rows >= col
+
+        def score(u, b):
+            i, m = units[u]
+            cut = slice(m * key_size, (m + 1) * key_size)
+            s = lax.dot_general(
+                q[i, :, cut], part(b, cut), (((1,), (1,)), ((), ())), preferred_element_type=jnp.float32
+            )
+            if b is None:
+                s = jnp.where(seen(i), s, HIDDEN)
+            held[u % 2, full if b is None else b] = s
+            top = s[:, :value_size]
+            for at in range(value_size, rows, value_size):
+                top = jnp.maximum(top, s[:, at : at + value_size])
+            return top
+
+        def peak(tops):
+            top = tops[0]
+            for t in tops[1:]:
+                top = jnp.maximum(top, t)
+            return jnp.max(top, axis=-1, keepdims=True)
+
         stats = []
-        for m in range(2):
-            query = queries[:, m * key_size : (m + 1) * key_size]
-            scores = []
-            for ref in chosen:
-                keys = ref[:, m * key_size : (m + 1) * key_size]
-                scores.append(
-                    lax.dot_general(query, keys, (((1,), (1,)), ((), ())), preferred_element_type=jnp.float32)
-                )
-            row = lax.broadcasted_iota(jnp.int32, (rows, rows), 0)
-            col = lax.broadcasted_iota(jnp.int32, (rows, rows), 1)
-            seen = row + ahead >= col
-            scores[-1] = jnp.where(seen, scores[-1], HIDDEN)
-            tops = [s[:, i : i + value_size] for s in scores for i in range(0, s.shape[1], value_size)]
-            top = tops[0]
-            for s in tops[1:]:
-                top = jnp.maximum(top, s)
-            top = jnp.max(top, axis=-1, keepdims=True)
+        top = peak([score(0, b) for b in order])
+        for u, (i, m) in enumerate(units):
+            ahead = []
             summed = jnp.zeros((rows, 2 * value_size), jnp.float32)
-            for ref, score in zip(chosen, scores):
-                w = jnp.exp2(score - top)
-                if ref is blocks[0]:
-                    w = jnp.where(seen, w, 0.0)
-                ones = jnp.ones((ref.shape[0], value_size), jnp.bfloat16)
-                values = jnp.concatenate([ref[:, value_size:], ones], axis=1)
+            for b in order:
+                if u + 1 < len(units):
+                    ahead.append(score(u + 1, b))
+                w = jnp.exp2(held[u % 2, full if b is None else b] - top)
+                if b is None:
+                    w = jnp.where(seen(i), w, 0.0)
+                values = jnp.concatenate([part(b, slice(value_size, None)), ones], axis=1)
                 summed = summed + jnp.dot(w.astype(jnp.bfloat16), values, preferred_element_type=jnp.float32)
             total = summed[:, value_size:]
             some = total > 0.0
             safe = jnp.where(some, total, 1.0)
-            out[0, :rows, m * value_size : (m + 1) * value_size] = (summed[:, :value_size] / safe).astype(
+            out[i, :rows, m * value_size : (m + 1) * value_size] = (summed[:, :value_size] / safe).astype(
                 jnp.bfloat16
             )
             stats.append(jnp.where(some, jnp.log2(safe) + top, HIDDEN))
-        lane = lax.broadcasted_iota(jnp.int32, (rows, value_size), 1)
-        spread = jnp.zeros((rows, value_size), jnp.float32)
-        for m in range(2):
-            rest = stats[m]
-            for piece in range(3):
-                rounded = rest.astype(jnp.bfloat16).astype(jnp.float32)
-                spread = jnp.where(lane == 2 * piece + m, rounded, spread)
-                rest = rest - rounded
-        turned = jnp.transpose(spread)
-        out[0, rows:, :] = turned[: out.shape[1] - rows].astype(jnp.bfloat16)
-
-    for used in range(1, len(blocks)):
-        pl.when(last == used - 1)(functools.partial(body, used))
+            if ahead:
+                top = peak(ahead)
+        for i in range(span):
+            spread = jnp.zeros((rows, value_size), jnp.float32)
+            for m in range(2):
+                rest = stats[2 * i + m]
+                for piece in range(3):
+                    rounded = rest.astype(jnp.bfloat16).astype(jnp.float32)
+                    spread = jnp.where(lane == 2 * piece + m, rounded, spread)
+                    rest = rest - rounded
+            turned = jnp.transpose(spread)
+            out[i, rows:, :] = turned[: out.shape[1] - rows].astype(jnp.bfloat16)
+
+    for full in range(kv.shape[0] + 1):
+        pl.when(last == full)(functools.partial(body, full))
 
 
 def finish_kernel(lam, parts, gate, conv, head_gain, attn_w, conv_w, mixed, totals):
@@ -148,7 +166,7 @@
 SMEM = pl.BlockSpec(memory_space=pltpu.SMEM)
 
 
-def project(core, own, other, gain, weights, copies):
+def project(own, other, gain, weights, copies):
     rows = own.shape[1]
     width = gain.shape[0]
     columns = weights[0].shape[1]
@@ -162,24 +180,30 @@
             narrow,
             narrow,
         ),
-        in_specs=[SMEM] + [VMEM] * 10,
+        in_specs=[VMEM] * 10,
         out_specs=(VMEM,) * 5,
         scratch_shapes=[pltpu.VMEM((rows, width), jnp.bfloat16)],
         name="project",
-    )(core.reshape(1), own, other, gain.reshape(1, width), *weights)
-
-
-def attend(place, queries, blocks, extra):
+    )(own, other, gain.reshape(1, width), *weights)
+
+
+def attend(queries, own, kv, chunk, extra):
     count, rows, columns = queries.shape
-    wide = blocks[0].shape[1]
+    others, _, wide = kv.shape
+    span = 2
+
+    def tiled(length, width):
+        return pl.BlockSpec((span, length, width), lambda i: (i, 0, 0))
+
     return pl.pallas_call(
-        attend_kernel,
-        grid=(count,),
+        functools.partial(attend_kernel, chunk, span),
+        grid=(count // span,),
         out_shape=jax.ShapeDtypeStruct((count, rows + extra, wide), jnp.bfloat16),
-        in_specs=[SMEM, pl.BlockSpec((1, rows, columns), lambda i: (i, 0, 0))] + [VMEM] * len(blocks),
-        out_specs=pl.BlockSpec((1, rows + extra, wide), lambda i: (i, 0, 0)),
+        in_specs=[tiled(rows, columns), VMEM, VMEM],
+        out_specs=tiled(rows + extra, wide),
+        scratch_shapes=[pltpu.VMEM((2, others + 1, rows, rows), jnp.float32)],
         name="attend",
-    )(place, queries, *blocks)
+    )(queries, own, kv)
 
 
 def finish(lambdas, parts, gate, conv, head_gain, attn_w, conv_w):
@@ -196,21 +220,17 @@
     )(lambdas, parts, gate, conv, head_gain.reshape(1, -1), attn_w, conv_w)
 
 
-def around(block, chunk):
+def earlier_blocks(block, groups, chunk):
     devices = lax.axis_size("sp")
     count = devices // chunk
-    half = block.shape[0] // 2
-
-    def moved(array, by):
-        return lax.ppermute(array, "sp", [(i, (i + by * chunk) % devices) for i in range(devices)])
-
-    ups, downs = [block], [block]
-    for _ in range(count // 2 - 1):
-        ups.append(moved(ups[-1], 1))
-        downs.append(moved(downs[-1], -1))
-    ups.append(moved(ups[-1][:half], 1))
-    downs.append(moved(downs[-1][half:], -1))
-    return ups + downs[:0:-1]
+    rows, wide = block.shape
+    step = rows // count
+    share = rows - step
+    before = lax.ppermute(block[step:], "sp", [(i, i + chunk) for i in range(devices - chunk)])
+    start = share - lax.div(lax.axis_index("sp"), chunk) * step
+    held = lax.dynamic_slice_in_dim(jnp.concatenate([before, block], axis=0), start, share, 0)
+    gathered = lax.all_gather(held, "sp", axis_index_groups=groups, tiled=True)
+    return gathered.reshape(count - 1, rows, wide)
 
 
 def convolve(outer, insig, taps):
@@ -245,14 +265,12 @@
     tp = lax.axis_size("tp")
     sp = lax.axis_size("sp")
     near = [[g * chunk + i for i in range(chunk)] for g in range(sp // chunk)]
+    far = [[g * chunk + i for g in range(sp // chunk)] for i in range(chunk)]
     same_core = [[2 * x + c for x in range(tp // 2)] for c in range(2)]
-    core = lax.rem(lax.axis_index("tp"), 2)
-    index = lax.axis_index("sp")
 
     own = lax.all_gather(tokens, "tp", axis_index_groups=same_core)
     other = lax.ppermute(own, "tp", [(i, i ^ 1) for i in range(tp)])
     kv, query, gate, outer, insig = project(
-        core,
         own,
         other,
         norm_gain,
@@ -260,10 +278,8 @@
         chunk,
     )
     queries = lax.all_to_all(query, "sp", 0, 0, axis_index_groups=near, tiled=True)
-    blocks = around(kv, chunk)
     conv = convolve(outer, insig, conv_taps)
-    place = jnp.stack([lax.div(index, chunk), lax.rem(index, chunk)]).astype(jnp.int32)
-    parts = attend(place, queries, blocks, 16)
+    parts = attend(queries, kv, earlier_blocks(kv, far, chunk), chunk, 16)
     parts = lax.all_to_all(parts, "sp", 0, 0, axis_index_groups=near, tiled=True)
     partial, log_totals = finish(lambdas, parts, gate, conv, head_gain, attn_out_weight, conv_out_weight)
     tiles = lax.all_to_all(partial.reshape(tp, -1, partial.shape[1]), "tp", 0, 0, tiled=True)

time: 142 us -> 135 us (0.951)
  blocking collectives: 33.3 us -> 67.2 us
  starting transfers between devices: 46.7 us -> 22.6 us
  waiting for transfers between devices: 23.5 us -> 15.1 us
  Pallas kernels: 30.3 us -> 23 us
    all_gather x0 -> x1, blocking collectives: none -> 34 us  [earlier_blocks(): gathered = lax.all_gather(held, 'sp', axis_index_groups=groups, tiled=True)]
    ppermute x8 -> x1, starting transfers between devices: 28.7 us -> 1.29 us  [earlier_blocks(): lax.ppermute(block[step:], 'sp', [(i, i + chunk) for i in range(devices -...]
    pallas_call x1, Pallas kernels: 20.7 us -> 13.3 us  [attend(): pl.pallas_call(functools.partial(attend_kernel, chunk, span), grid=(count...]
    ppermute x8 -> x1, waiting for transfers between devices: 13.7 us -> 6.58 us  [earlier_blocks(): lax.ppermute(block[step:], 'sp', [(i, i + chunk) for i in range(devices -...]
    all_to_all x1, starting transfers between devices: 6.78 us -> 9.99 us  [per_device(): lax.all_to_all(parts, 'sp', 0, 0, axis_index_groups=near, tiled=True)]
    unnamed x30 -> x16, local copies, waits for them, and re-layouts: 3.2 us -> 2.64 us
  transfers between devices with their start and end apart: 12 -> 5, of which waited for: 7 -> 3; matrix products, arithmetic and copies ran while one was open for 1% -> 1% of each run, Pallas kernels for 0% -> 0%
where the time goes in v3:
time: 135 us; the launch traced here: 134 us
  blocking collectives  67.2 us (50%)
  Pallas kernels  23 us (17%)
  starting transfers between devices  22.6 us (17%)
  waiting for transfers between devices  15.1 us (11%)
  local copies, waits for them, and re-layouts  2.66 us (2%)
  other arithmetic  1.75 us (1%)
  between operations  1.37 us (1%)
    all_gather x1, blocking collectives, earlier_blocks(): gathered = lax.all_gather(held, 'sp', axis_index_groups=groups, tiled=True)  34 us
    all_to_all x1, blocking collectives, per_device(): lax.all_to_all(partial.reshape(tp, -1, partial.shape[1]), 'tp', 0, 0, til...  19.9 us
    all_gather x1, blocking collectives, per_device(): own = lax.all_gather(tokens, 'tp', axis_index_groups=same_core)  13.3 us
    pallas_call x1, Pallas kernels, attend(): pl.pallas_call(functools.partial(attend_kernel, chunk, span), grid=(count...  13.3 us
    all_to_all x1, starting transfers between devices, per_device(): lax.all_to_all(parts, 'sp', 0, 0, axis_index_groups=near, tiled=True)  9.99 us
    ppermute x1, waiting for transfers between devices, convolve(): lax.ppermute(insig[rows - reach:], 'sp', [(i, i + 1) for i in range(count...  6.68 us
    ppermute x1, waiting for transfers between devices, earlier_blocks(): lax.ppermute(block[step:], 'sp', [(i, i + chunk) for i in range(devices -...  6.58 us
    all_to_all x1, starting transfers between devices, per_device(): lax.all_to_all(query, 'sp', 0, 0, axis_index_groups=near, tiled=True)  6.07 us
  transfers between devices with their start and end apart: 5, of which 3 were waited for; matrix products, arithmetic and copies ran while one was open for 1% of the time, Pallas kernels for 0%

profile of v3, /device:TPU:480, one launch (start us, length us, event | category | flops | bytes accessed | tf_op | source)
XLA Modules:
  0.0 133.7 jit_solution(2582941835724526707)
XLA Ops:
  0.6 13.3 %all-gather = bf16[1024,256]{1,0:T(8,128)(2,1)S(1)} all-gather(bf16[256,256]{1,0:T(8,128)(2,1)} %param.14), channel_id=2, replica_groups={{0,2,4,6},{1,3,5,7},{8,10,12,14},{9,11,13,15},{16,18,20,22},{17,19,21,2..., dimensions={0}, use_global_device_ids=true | all-gather | bytes 655360 | tf_op jit(solution)/shard_map/all_gather | solution.py:271
  14.0 0.0 copy-start.1
  14.0 1.9 %collective-permute-start = (bf16[4,256,256]{2,1,0:T(8,128)(2,1)S(1)}, bf16[4,256,256]{2,1,0:T(8,128)(2,1)S(1)}, u32[]{:S(2)}, u32[]{:S(2)}) collective-permute-start(bf16[4,256,256]{2,1,0:T(8,128)(2,1)S(1)} %bitcast.12), channel_id=1, source_target_pairs={{0,1},{1,0},{2,3},{3,2},{4,5},{5,4},{6,7},{7,6},{8,9},{9,8},{10,11... | collective-permute-start | bytes 1572872 | tf_op jit(solution)/shard_map/ppermute | solution.py:272
  15.9 1.9 %collective-permute-done.other = bf16[4,256,256]{2,1,0:T(8,128)(2,1)S(1)} collective-permute-done((bf16[4,256,256]{2,1,0:T(8,128)(2,1)S(1)}, bf16[4,256,256]{2,1,0:T(8,128)(2,1)S(1)}, u32[]{:S(2)}, u32[]{:S(2)}) %collective-permute-start) | collective-permute-done | bytes 524320 | tf_op jit(solution)/shard_map/ppermute | solution.py:272
  17.8 0.0 copy-start.4
  17.8 0.0 copy-done.1
  17.8 0.8 copy-done.4
  18.6 5.4 %project.1 = (bf16[256,256]{1,0:T(8,128)(2,1)}, bf16[8,256,128]{2,1,0:T(8,128)(2,1)}, bf16[256,128]{1,0:T(8,128)(2,1)}, bf16[256,128]{1,0:T(8,128)(2,1)}, bf16[256,128]{1,0:T(8,128)(2,1)}) custom-call(bf16[4,256,256]{2,1,0:T(8,128)(2,1)} %bitcast.13, bf16[4,256,256]{2,1,0:T(8,128)(2,1)} %copy-done.4, f32[1,2048]{1,0:T(1,128)} %bitcast.15, ...), custom_call_target="tpu_custom_call" | custom-call | tf_op jit(solution)/shard_map/project/pallas_call | solution.py:174
  24.0 0.0 copy-start.3
  24.0 6.1 %all-to-all-start = ((bf16[8,256,128]{2,1,0:T(8,128)(2,1)}), bf16[8,256,128]{2,1,0:T(8,128)(2,1)S(1)}, u32[]{:S(2)}, u32[]{:S(2)}) async-start(bf16[8,256,128]{2,1,0:T(8,128)(2,1)} %get-tuple-element.9), calls=%async_computation | async-start | bytes 1048576 | tf_op jit(solution)/shard_map/all_to_all | solution.py:280
  30.1 0.0 copy-done.3
  30.1 1.3 collective-permute-start.1
  31.4 6.6 %collective-permute-done.1 = bf16[224,256]{1,0:T(8,128)(2,1)S(1)} collective-permute-done((bf16[224,256]{1,0:T(8,128)(2,1)S(1)}, bf16[224,256]{1,0:T(8,128)(2,1)S(1)}, u32[]{:S(2)}, u32[]{:S(2)}) %collective-permute-start.1) | collective-permute-done | bytes 114720 | tf_op jit(solution)/shard_map/ppermute | solution.py:229
  38.0 0.2 fusion.4
  38.2 34.0 %all_gather.11 = bf16[1792,256]{1,0:T(8,128)(2,1)} all-gather(bf16[224,256]{1,0:T(8,128)(2,1)S(1)} %fusion.4), channel_id=1, replica_groups={{0,64,128,192,256,320,384,448},{8,72,136,200,264,328,392,456},{16,80,14..., dimensions={0}, use_global_device_ids=true | all-gather | bytes 1032192 | tf_op jit(solution)/shard_map/all_gather | solution.py:232
  72.2 0.0 all-to-all-done.q
  72.2 0.0 copy-start.2
  72.2 0.8 copy-done.2
  73.0 13.3 %attend.1 = bf16[8,272,256]{2,1,0:T(8,128)(2,1)} custom-call(bf16[8,256,128]{2,1,0:T(8,128)(2,1)} %copy-done.2, bf16[256,256]{1,0:T(8,128)(2,1)} %get-tuple-element.10.own, bf16[7,256,256]{2,1,0:T(8,128)(2,1)} %bitcast.11), custom_call_target="tpu_custom_call" | custom-call | tf_op jit(solution)/shard_map/attend/pallas_call | solution.py:198
  86.3 0.0 copy-start.6
  86.3 10.0 %all-to-all-start.1 = ((bf16[8,272,256]{2,1,0:T(8,128)(2,1)}), bf16[8,272,256]{2,1,0:T(8,128)(2,1)S(1)}, u32[]{:S(2)}, u32[]{:S(2)}) async-start(bf16[8,272,256]{2,1,0:T(8,128)(2,1)} %attend.1), calls=%async_computation.1 | async-start | bytes 2228224 | tf_op jit(solution)/shard_map/all_to_all | solution.py:283
  96.3 0.0 copy-done.6
  96.3 3.4 %collective-permute-start.2 = (bf16[2,128]{1,0:T(2,128)(2,1)S(1)}, bf16[2,128]{1,0:T(2,128)(2,1)S(1)}, u32[]{:S(2)}, u32[]{:S(2)}) collective-permute-start(bf16[2,128]{1,0:T(2,128)(2,1)S(1)} %slice.26), channel_id=1, source_target_pairs={{0,8},{8,16},{16,24},{24,32},{32,40},{40,48},{48,56},{56,64},{64,7... | collective-permute-start | bytes 1544 | tf_op jit(solution)/shard_map/ppermute | solution.py:240
  99.7 0.0 copy-done.7
  100.3 6.7 %collective-permute-done.2 = bf16[2,128]{1,0:T(2,128)(2,1)S(1)} collective-permute-done((bf16[2,128]{1,0:T(2,128)(2,1)S(1)}, bf16[2,128]{1,0:T(2,128)(2,1)S(1)}, u32[]{:S(2)}, u32[]{:S(2)}) %collective-permute-start.2) | collective-permute-done | bytes 544 | tf_op jit(solution)/shard_map/ppermute | solution.py:240
  107.0 0.0 copy-done.5
  107.1 0.7 fusion.2.conv
  107.7 0.0 all-to-all-done.1.parts
  107.7 1.0 copy-done
  108.7 4.3 %finish.1 = (bf16[256,2048]{1,0:T(8,128)(2,1)}, f32[1,2,256]{2,1,0:T(2,128)}) custom-call(f32[1]{0:T(128)S(6)} %copy.16.lam, bf16[8,272,256]{2,1,0:T(8,128)(2,1)} %copy-done, bf16[256,128]{1,0:T(8,128)(2,1)} %get-tuple-element.11.gate, bf16[256,128]{1,0:T(8,128)(2,1)} %fusion.2.conv, f32[1,128]{1,0:T(1,128)} %bitcast.16, bf16[128,2048]{1,0:T(8,128)(2,1)} %attn_w.1, ...), custom_call_target="tpu_custom_call" | custom-call | tf_op jit(solution)/shard_map/finish/pallas_call | solution.py:211
  113.0 19.9 %all_to_all.15 = bf16[8,32,2048]{2,1,0:T(8,128)(2,1)S(1)} all-to-all(bf16[8,32,2048]{2,1,0:T(8,128)(2,1)} %bitcast.14), channel_id=1, replica_groups=mesh['sp'=64,'tp'=8] {'tp'}, dimensions={0} | all-to-all | bytes 2097152 | tf_op jit(solution)/shard_map/all_to_all | solution.py:285
  132.9 0.8 reduce_sum.12
  (7 shorter events, 0.0 us)
Async XLA Ops:
  14.0 3.8 %copy-start.1 = (bf16[1024,256]{1,0:T(8,128)(2,1)}, bf16[1024,256]{1,0:T(8,128)(2,1)S(1)}, u32[]{:S(2)}) copy-start(bf16[1024,256]{1,0:T(8,128)(2,1)S(1)} %all-gather) | copy-start | bytes 1572868
  14.0 3.8 %collective-permute-start = (bf16[4,256,256]{2,1,0:T(8,128)(2,1)S(1)}, bf16[4,256,256]{2,1,0:T(8,128)(2,1)S(1)}, u32[]{:S(2)}, u32[]{:S(2)}) collective-permute-start(bf16[4,256,256]{2,1,0:T(8,128)(2,1)S(1)} %bitcast.12), channel_id=1, source_target_pairs={{0,1},{1,0},{2,3},{3,2},{4,5},{5,4},{6,7},{7,6},{8,9},{9,8},{10,11... | collective-permute-start | bytes 1572872 | tf_op jit(solution)/shard_map/ppermute | solution.py:272
  17.8 0.8 copy-start.4
  24.0 6.1 %copy-start.3 = (bf16[256,256]{1,0:T(8,128)(2,1)S(1)}, bf16[256,256]{1,0:T(8,128)(2,1)}, u32[]{:S(2)}) copy-start(bf16[256,256]{1,0:T(8,128)(2,1)} %get-tuple-element.10.own) | copy-start | bytes 393220
  24.0 48.2 %all-to-all-start = ((bf16[8,256,128]{2,1,0:T(8,128)(2,1)}), bf16[8,256,128]{2,1,0:T(8,128)(2,1)S(1)}, u32[]{:S(2)}, u32[]{:S(2)}) async-start(bf16[8,256,128]{2,1,0:T(8,128)(2,1)} %get-tuple-element.9), calls=%async_computation | async-start | bytes 1048576 | tf_op jit(solution)/shard_map/all_to_all | solution.py:280
  30.1 7.9 %collective-permute-start.1 = (bf16[224,256]{1,0:T(8,128)(2,1)S(1)}, bf16[224,256]{1,0:T(8,128)(2,1)S(1)}, u32[]{:S(2)}, u32[]{:S(2)}) collective-permute-start(bf16[224,256]{1,0:T(8,128)(2,1)S(1)} %slice.24), channel_id=1, source_target_pairs={{0,64},{8,72},{16,80},{24,88},{32,96},{40,104},{48,112},{56,120},{... | collective-permute-start | bytes 344072 | tf_op jit(solution)/shard_map/ppermute | solution.py:229
  72.2 0.8 copy-start.2
  86.3 10.0 %copy-start.6 = (bf16[256,128]{1,0:T(8,128)(2,1)S(1)}, bf16[256,128]{1,0:T(8,128)(2,1)}, u32[]{:S(2)}) copy-start(bf16[256,128]{1,0:T(8,128)(2,1)} %get-tuple-element.13) | copy-start | bytes 196612
  86.3 13.4 %copy-start.7 = (f32[3,128]{1,0:T(4,128)S(1)}, f32[3,128]{1,0:T(4,128)}, u32[]{:S(2)}) copy-start(f32[3,128]{1,0:T(4,128)} %param.23) | copy-start | bytes 4612
  86.3 20.8 %copy-start.5 = (bf16[256,128]{1,0:T(8,128)(2,1)S(1)}, bf16[256,128]{1,0:T(8,128)(2,1)}, u32[]{:S(2)}) copy-start(bf16[256,128]{1,0:T(8,128)(2,1)} %get-tuple-element.12) | copy-start | bytes 196612
  86.3 21.4 %all-to-all-start.1 = ((bf16[8,272,256]{2,1,0:T(8,128)(2,1)}), bf16[8,272,256]{2,1,0:T(8,128)(2,1)S(1)}, u32[]{:S(2)}, u32[]{:S(2)}) async-start(bf16[8,272,256]{2,1,0:T(8,128)(2,1)} %attend.1), calls=%async_computation.1 | async-start | bytes 2228224 | tf_op jit(solution)/shard_map/all_to_all | solution.py:283
  96.3 10.7 %collective-permute-start.2 = (bf16[2,128]{1,0:T(2,128)(2,1)S(1)}, bf16[2,128]{1,0:T(2,128)(2,1)S(1)}, u32[]{:S(2)}, u32[]{:S(2)}) collective-permute-start(bf16[2,128]{1,0:T(2,128)(2,1)S(1)} %slice.26), channel_id=1, source_target_pairs={{0,8},{8,16},{16,24},{24,32},{32,40},{40,48},{48,56},{56,64},{64,7... | collective-permute-start | bytes 1544 | tf_op jit(solution)/shard_map/ppermute | solution.py:240
  107.7 1.0 copy-start

commit v4 on v3

--- a/solution.py
+++ b/solution.py
@@ -7,14 +7,16 @@
 from jax.experimental.pallas import tpu as pltpu
 from jax.sharding import PartitionSpec as P
 
+
 LOG2E = 1.4426950408889634
 LN2 = 0.6931471805599453
 HIDDEN = -1e30
 
 
-def project_kernel(own, other, gain, qw, kw, vw, gw, ow, iw, sw, kv, q, gate, outer, insig, normed):
+def project_kernel(own, other, gain, qw, kw, vw, iw, sw, kv, q, normed, scaled):
     count, rows, part = own.shape
     width = normed.shape[1]
+    tail = kv.shape[0] - rows
 
     def spread(core):
         squares = jnp.zeros((rows, part), jnp.float32)
@@ -26,28 +28,40 @@
                 normed[:, at : at + part] = (piece * gain[:, at : at + part]).astype(jnp.bfloat16)
         scale = lax.rsqrt(jnp.sum(squares, axis=-1, keepdims=True) / width + 1e-06)
 
-        def project(weight, factor=None):
-            raw = jnp.dot(normed[...], weight[...], preferred_element_type=jnp.float32)
-            raw = raw * scale
+        def project(weight, low=0, factor=None):
+            raw = jnp.dot(normed[low:, :], weight[...], preferred_element_type=jnp.float32)
+            raw = raw * scale[low:]
             if factor is not None:
                 raw = raw * factor
             return raw.astype(jnp.bfloat16)
 
         columns = kw.shape[1]
-        kv[:, :columns] = project(kw)
-        kv[:, columns:] = project(vw)
-        query = project(qw, LOG2E * (columns // 2) ** -0.5)
+        kv[:rows, :columns] = project(kw)
+        kv[:rows, columns:] = project(vw)
+        low = rows - tail
+        ending = project(iw, low).astype(jnp.float32) * project(sw, low).astype(jnp.float32)
+        kv[rows:, :columns] = ending.astype(jnp.bfloat16)
+        kv[rows:, columns:] = jnp.zeros((tail, columns), jnp.bfloat16)
+        query = project(qw, 0, LOG2E * (columns // 2) ** -0.5)
         for i in range(q.shape[0]):
             q[i] = query
-        insig[...] = (project(iw).astype(jnp.float32) * project(sw).astype(jnp.float32)).astype(jnp.bfloat16)
-        outer[...] = project(ow)
-        gate[...] = project(gw)
+        scaled[...] = jnp.broadcast_to(scale, scaled.shape)
 
     for core in range(2):
         pl.when(lax.rem(lax.axis_index("tp"), 2) == core)(functools.partial(spread, core))
 
 
-def attend_kernel(chunk, span, q, own, kv, out, held):
+def gates_kernel(normed, scale, gw, ow, iw, sw, gate, outer, insig):
+    def project(weight):
+        raw = jnp.dot(normed[...], weight[...], preferred_element_type=jnp.float32)
+        return (raw * scale[...]).astype(jnp.bfloat16)
+
+    insig[...] = (project(iw).astype(jnp.float32) * project(sw).astype(jnp.float32)).astype(jnp.bfloat16)
+    outer[...] = project(ow)
+    gate[...] = project(gw)
+
+
+def attend_kernel(chunk, span, q, own, kv, ending, out, held):
     rows = q.shape[1]
     columns = kv.shape[2]
     value_size = columns // 2
@@ -66,7 +80,7 @@
         col = lax.broadcasted_iota(jnp.int32, (rows, rows), 1)
 
         def part(b, cut):
-            return own[:, cut] if b is None else kv[b, :, cut]
+            return own[:rows, cut] if b is None else kv[b, :, cut]
 
         def seen(i):
             return row + (first + i - slot) * rows >= col
@@ -121,14 +135,17 @@
                     rounded = rest.astype(jnp.bfloat16).astype(jnp.float32)
                     spread = jnp.where(lane == 2 * piece + m, rounded, spread)
                     rest = rest - rounded
-            turned = jnp.transpose(spread)
-            out[i, rows:, :] = turned[: out.shape[1] - rows].astype(jnp.bfloat16)
+            tail = out.shape[1] - rows
+            turned = jnp.transpose(spread)[:tail].astype(jnp.bfloat16)
+            ends = jnp.concatenate([own[rows:, :value_size], ending[:, :value_size]], axis=1)
+            line = lax.broadcasted_iota(jnp.int32, (tail, columns), 0)
+            out[i, rows:, :] = jnp.where(line < tail // 2, turned, ends)
 
     for full in range(kv.shape[0] + 1):
         pl.when(last == full)(functools.partial(body, full))
 
 
-def finish_kernel(lam, parts, gate, conv, head_gain, attn_w, conv_w, mixed, totals):
+def finish_kernel(lam, parts, gate, outer, insig, taps, head_gain, attn_w, conv_w, mixed, totals):
     count, _, columns = parts.shape
     rows = gate.shape[0]
     value_size = columns // 2
@@ -156,9 +173,23 @@
     norm = lax.rsqrt(jnp.mean(diff * diff, axis=-1, keepdims=True) + 1e-05)
     opened = gate[...].astype(jnp.float32)
     head = diff * norm * head_gain[...] * (opened / (1.0 + jnp.exp(-opened)))
+    slot = lax.rem(lax.axis_index("sp"), count)
+    ends = parts[lax.rem(slot + count - 1, count), rows:, :].astype(jnp.float32)
+    ends = jnp.where(slot == 0, ends[:, value_size:], ends[:, :value_size])
+    reach = taps.shape[0] - 1
+    signal = insig[...].astype(jnp.float32)
+    row = lax.broadcasted_iota(jnp.int32, signal.shape, 0)
+    convolved = taps[reach : reach + 1, :] * signal
+    for by in range(1, reach + 1):
+        moved = pltpu.roll(signal, by, axis=0)
+        for at in range(by):
+            line = ends.shape[0] - by + at
+            moved = jnp.where(row == at, ends[line : line + 1, :], moved)
+        convolved = convolved + taps[reach - by : reach - by + 1, :] * moved
+    conv = (outer[...].astype(jnp.float32) * convolved).astype(jnp.bfloat16)
     mixed[...] = (
         jnp.dot(head.astype(jnp.bfloat16), attn_w[...], preferred_element_type=jnp.float32)
-        + jnp.dot(conv[...], conv_w[...], preferred_element_type=jnp.float32)
+        + jnp.dot(conv, conv_w[...], preferred_element_type=jnp.float32)
     ).astype(jnp.bfloat16)
 
 
@@ -166,30 +197,40 @@
 SMEM = pl.BlockSpec(memory_space=pltpu.SMEM)
 
 
-def project(own, other, gain, weights, copies):
+def project(own, other, gain, weights, copies, tail):
     rows = own.shape[1]
     width = gain.shape[0]
     columns = weights[0].shape[1]
-    narrow = jax.ShapeDtypeStruct((rows, columns), jnp.bfloat16)
     return pl.pallas_call(
         project_kernel,
         out_shape=(
-            jax.ShapeDtypeStruct((rows, 2 * columns), jnp.bfloat16),
+            jax.ShapeDtypeStruct((rows + tail, 2 * columns), jnp.bfloat16),
             jax.ShapeDtypeStruct((copies, rows, columns), jnp.bfloat16),
-            narrow,
-            narrow,
-            narrow,
+            jax.ShapeDtypeStruct((rows, width), jnp.bfloat16),
+            jax.ShapeDtypeStruct((rows, columns), jnp.float32),
         ),
-        in_specs=[VMEM] * 10,
-        out_specs=(VMEM,) * 5,
-        scratch_shapes=[pltpu.VMEM((rows, width), jnp.bfloat16)],
+        in_specs=[VMEM] * 8,
+        out_specs=(VMEM,) * 4,
         name="project",
     )(own, other, gain.reshape(1, width), *weights)
 
 
-def attend(queries, own, kv, chunk, extra):
+def gates(normed, scale, weights):
+    shape = jax.ShapeDtypeStruct((normed.shape[0], weights[0].shape[1]), jnp.bfloat16)
+    return pl.pallas_call(
+        gates_kernel,
+        out_shape=(shape,) * 3,
+        in_specs=[VMEM] * 6,
+        out_specs=(VMEM,) * 3,
+        cost_estimate=pl.CostEstimate(flops=8 * normed.size * weights[0].shape[1], transcendentals=0, bytes_accessed=4 * normed.size),
+        name="gates",
+    )(normed, scale, *weights)
+
+
+def attend(queries, own, kv, ending, chunk):
     count, rows, columns = queries.shape
     others, _, wide = kv.shape
+    extra = ending.shape[0]
     span = 2
 
     def tiled(length, width):
@@ -199,14 +240,14 @@
         functools.partial(attend_kernel, chunk, span),
         grid=(count // span,),
         out_shape=jax.ShapeDtypeStruct((count, rows + extra, wide), jnp.bfloat16),
-        in_specs=[tiled(rows, columns), VMEM, VMEM],
+        in_specs=[tiled(rows, columns), VMEM, VMEM, VMEM],
         out_specs=tiled(rows + extra, wide),
         scratch_shapes=[pltpu.VMEM((2, others + 1, rows, rows), jnp.float32)],
         name="attend",
-    )(queries, own, kv)
-
-
-def finish(lambdas, parts, gate, conv, head_gain, attn_w, conv_w):
+    )(queries, own, kv, ending)
+
+
+def finish(lambdas, parts, gate, outer, insig, taps, head_gain, attn_w, conv_w):
     rows = gate.shape[0]
     return pl.pallas_call(
         finish_kernel,
@@ -214,35 +255,23 @@
             jax.ShapeDtypeStruct((rows, attn_w.shape[1]), jnp.bfloat16),
             jax.ShapeDtypeStruct((1, 2, rows), jnp.float32),
         ),
-        in_specs=[SMEM] + [VMEM] * 6,
+        in_specs=[SMEM] + [VMEM] * 8,
         out_specs=(VMEM, VMEM),
         name="finish",
-    )(lambdas, parts, gate, conv, head_gain.reshape(1, -1), attn_w, conv_w)
-
-
-def earlier_blocks(block, groups, chunk):
+    )(lambdas, parts, gate, outer, insig, taps, head_gain.reshape(1, -1), attn_w, conv_w)
+
+
+def earlier_blocks(block, groups, chunk, tail):
     devices = lax.axis_size("sp")
     count = devices // chunk
-    rows, wide = block.shape
+    rows, wide = block.shape[0] - tail, block.shape[1]
     step = rows // count
     share = rows - step
     before = lax.ppermute(block[step:], "sp", [(i, i + chunk) for i in range(devices - chunk)])
     start = share - lax.div(lax.axis_index("sp"), chunk) * step
-    held = lax.dynamic_slice_in_dim(jnp.concatenate([before, block], axis=0), start, share, 0)
+    held = lax.dynamic_slice_in_dim(jnp.concatenate([before[:share], block[:rows]], axis=0), start, share, 0)
     gathered = lax.all_gather(held, "sp", axis_index_groups=groups, tiled=True)
-    return gathered.reshape(count - 1, rows, wide)
-
-
-def convolve(outer, insig, taps):
-    rows = insig.shape[0]
-    reach = taps.shape[0] - 1
-    count = lax.axis_size("sp")
-    before = lax.ppermute(insig[rows - reach :], "sp", [(i, i + 1) for i in range(count - 1)])
-    extended = jnp.concatenate([before, insig], axis=0).astype(jnp.float32)
-    summed = jnp.zeros(insig.shape, jnp.float32)
-    for j in range(reach + 1):
-        summed = summed + taps[j] * extended[j : j + rows]
-    return (outer.astype(jnp.float32) * summed).astype(jnp.bfloat16)
+    return gathered.reshape(count - 1, rows, wide), before[share:]
 
 
 def per_device(
@@ -270,18 +299,24 @@
 
     own = lax.all_gather(tokens, "tp", axis_index_groups=same_core)
     other = lax.ppermute(own, "tp", [(i, i ^ 1) for i in range(tp)])
-    kv, query, gate, outer, insig = project(
+    tail = 16
+    kv, query, normed, scale = project(
         own,
         other,
         norm_gain,
-        (query_weight, key_weight, value_weight, gate_weight, outer_weight, inner_weight, signal_weight),
+        (query_weight, key_weight, value_weight, inner_weight, signal_weight),
         chunk,
+        tail,
     )
     queries = lax.all_to_all(query, "sp", 0, 0, axis_index_groups=near, tiled=True)
-    conv = convolve(outer, insig, conv_taps)
-    parts = attend(queries, kv, earlier_blocks(kv, far, chunk), chunk, 16)
+    earlier, ending = earlier_blocks(kv, far, chunk, tail)
+    parts = attend(queries, kv, earlier, ending, chunk)
+    normed, parts = lax.optimization_barrier((normed, parts))
+    gate, outer, insig = gates(normed, scale, (gate_weight, outer_weight, inner_weight, signal_weight))
     parts = lax.all_to_all(parts, "sp", 0, 0, axis_index_groups=near, tiled=True)
-    partial, log_totals = finish(lambdas, parts, gate, conv, head_gain, attn_out_weight, conv_out_weight)
+    partial, log_totals = finish(
+        lambdas, parts, gate, outer, insig, conv_taps, head_gain, attn_out_weight, conv_out_weight
+    )
     tiles = lax.all_to_all(partial.reshape(tp, -1, partial.shape[1]), "tp", 0, 0, tiled=True)
     mixed = jnp.sum(tiles.astype(jnp.float32), axis=0).astype(jnp.bfloat16)
     return mixed, log_totals
@@ -304,6 +339,7 @@
         P("tp", None),
         P("tp", None),
     )
+
     return jax.shard_map(
         per_device,
         mesh=mesh,

time: 135 us -> 134 us (level)
  starting transfers between devices: 22.6 us -> 19.5 us
  Pallas kernels: 23 us -> 25.9 us
    ppermute x1 -> x0, waiting for transfers between devices: 6.68 us -> none  [convolve(): lax.ppermute(insig[rows - reach:], 'sp', [(i, i + 1) for i in range(count...]
    all_to_all x1, waiting for transfers between devices: 0.01 us -> 5.96 us  [per_device(): lax.all_to_all(parts, 'sp', 0, 0, axis_index_groups=near, tiled=True)]
    ppermute x1 -> x0, starting transfers between devices: 3.37 us -> none  [convolve(): lax.ppermute(insig[rows - reach:], 'sp', [(i, i + 1) for i in range(count...]
    pallas_call x1 -> x2, Pallas kernels: 5.4 us -> 8.26 us  [the longest x1 4.49 us: project(): pl.pallas_call(project_kernel, out_shape=(jax.ShapeDtypeStruct((rows + ta...]
  transfers between devices with their start and end apart: 5 -> 4, of which waited for: 3 -> 3; matrix products, arithmetic and copies ran while one was open for 1% -> 1% of each run, Pallas kernels for 0% -> 3%
where the time goes in v4:
time: 134 us; the launch traced here: 133 us
  blocking collectives  67.4 us (50%)
  Pallas kernels  25.9 us (19%)
  starting transfers between devices  19.5 us (15%)
  waiting for transfers between devices  14.5 us (11%)
  local copies, waits for them, and re-layouts  3.22 us (2%)
  between operations  1.34 us (1%)
    all_gather x1, blocking collectives, earlier_blocks(): gathered = lax.all_gather(held, 'sp', axis_index_groups=groups, tiled=True)  34 us
    all_to_all x1, blocking collectives, per_device(): lax.all_to_all(partial.reshape(tp, -1, partial.shape[1]), 'tp', 0, 0, til...  20 us
    all_gather x1, blocking collectives, per_device(): own = lax.all_gather(tokens, 'tp', axis_index_groups=same_core)  13.3 us
    pallas_call x1, Pallas kernels, attend(): pl.pallas_call(functools.partial(attend_kernel, chunk, span), grid=(count...  13.3 us
    all_to_all x1, starting transfers between devices, per_device(): lax.all_to_all(parts, 'sp', 0, 0, axis_index_groups=near, tiled=True)  10.2 us
    ppermute x1, waiting for transfers between devices, earlier_blocks(): lax.ppermute(block[step:], 'sp', [(i, i + chunk) for i in range(devices -...  6.64 us
    all_to_all x1, starting transfers between devices, per_device(): lax.all_to_all(query, 'sp', 0, 0, axis_index_groups=near, tiled=True)  6.06 us
    all_to_all x1, waiting for transfers between devices, per_device(): lax.all_to_all(parts, 'sp', 0, 0, axis_index_groups=near, tiled=True)  5.96 us
  transfers between devices with their start and end apart: 4, of which 3 were waited for; matrix products, arithmetic and copies ran while one was open for 1% of the time, Pallas kernels for 3%

profile of v4, /device:TPU:480, one launch (start us, length us, event | category | flops | bytes accessed | tf_op | source)
XLA Modules:
  0.0 132.9 jit_solution(2205384204262004072)
XLA Ops:
  0.6 13.3 %all-gather = bf16[1024,256]{1,0:T(8,128)(2,1)S(1)} all-gather(bf16[256,256]{1,0:T(8,128)(2,1)} %param.14), channel_id=2, replica_groups={{0,2,4,6},{1,3,5,7},{8,10,12,14},{9,11,13,15},{16,18,20,22},{17,19,21,2..., dimensions={0}, use_global_device_ids=true | all-gather | bytes 655360 | tf_op jit(solution)/shard_map/all_gather | solution.py:300
  14.0 0.0 copy-start.1
  14.0 1.9 %collective-permute-start = (bf16[4,256,256]{2,1,0:T(8,128)(2,1)S(1)}, bf16[4,256,256]{2,1,0:T(8,128)(2,1)S(1)}, u32[]{:S(2)}, u32[]{:S(2)}) collective-permute-start(bf16[4,256,256]{2,1,0:T(8,128)(2,1)S(1)} %bitcast.6), channel_id=1, source_target_pairs={{0,1},{1,0},{2,3},{3,2},{4,5},{5,4},{6,7},{7,6},{8,9},{9,8},{10,11... | collective-permute-start | bytes 1572872 | tf_op jit(solution)/shard_map/ppermute | solution.py:301
  15.9 1.9 %collective-permute-done.other = bf16[4,256,256]{2,1,0:T(8,128)(2,1)S(1)} collective-permute-done((bf16[4,256,256]{2,1,0:T(8,128)(2,1)S(1)}, bf16[4,256,256]{2,1,0:T(8,128)(2,1)S(1)}, u32[]{:S(2)}, u32[]{:S(2)}) %collective-permute-start) | collective-permute-done | bytes 524320 | tf_op jit(solution)/shard_map/ppermute | solution.py:301
  17.8 0.0 copy-start.4
  17.8 0.0 copy-done.1
  17.8 0.8 copy-done.4
  18.6 4.5 %project.1 = (bf16[272,256]{1,0:T(8,128)(2,1)}, bf16[8,256,128]{2,1,0:T(8,128)(2,1)}, bf16[256,2048]{1,0:T(8,128)(2,1)}, f32[256,128]{1,0:T(8,128)}) custom-call(bf16[4,256,256]{2,1,0:T(8,128)(2,1)} %bitcast.7, bf16[4,256,256]{2,1,0:T(8,128)(2,1)} %copy-done.4, f32[1,2048]{1,0:T(1,128)} %bitcast.9, bf16[2048,128]{1,0:T(8,128)(2,1)} %qw.1, ...), custom_call_target="tpu_custom_call" | custom-call | tf_op jit(solution)/shard_map/project/pallas_call | solution.py:204
  23.1 0.0 copy-start.3
  23.1 6.1 %all-to-all-start = ((bf16[8,256,128]{2,1,0:T(8,128)(2,1)}), bf16[8,256,128]{2,1,0:T(8,128)(2,1)S(1)}, u32[]{:S(2)}, u32[]{:S(2)}) async-start(bf16[8,256,128]{2,1,0:T(8,128)(2,1)} %get-tuple-element.14), calls=%async_computation | async-start | bytes 1048576 | tf_op jit(solution)/shard_map/all_to_all | solution.py:311
  29.1 0.0 copy-done.3
  29.1 1.3 collective-permute-start.1
  30.5 6.6 %collective-permute-done.1 = bf16[240,256]{1,0:T(8,128)(2,1)S(1)} collective-permute-done((bf16[240,256]{1,0:T(8,128)(2,1)S(1)}, bf16[240,256]{1,0:T(8,128)(2,1)S(1)}, u32[]{:S(2)}, u32[]{:S(2)}) %collective-permute-start.1) | collective-permute-done | bytes 122912 | tf_op jit(solution)/shard_map/ppermute | solution.py:270
  37.1 0.6 slice.17.ending
  37.7 0.2 fusion
  38.0 34.0 %all_gather.11 = bf16[1792,256]{1,0:T(8,128)(2,1)} all-gather(bf16[224,256]{1,0:T(8,128)(2,1)S(1)} %fusion), channel_id=1, replica_groups={{0,64,128,192,256,320,384,448},{8,72,136,200,264,328,392,456},{16,80,14..., dimensions={0}, use_global_device_ids=true | all-gather | bytes 1032192 | tf_op jit(solution)/shard_map/all_gather | solution.py:273
  72.0 0.0 all-to-all-done.q
  72.0 0.0 copy-start.2
  72.0 0.8 copy-done.2
  72.8 13.3 %attend.1 = bf16[8,272,256]{2,1,0:T(8,128)(2,1)} custom-call(bf16[8,256,128]{2,1,0:T(8,128)(2,1)} %copy-done.2, bf16[272,256]{1,0:T(8,128)(2,1)} %get-tuple-element.15.own, bf16[7,256,256]{2,1,0:T(8,128)(2,1)} %bitcast.5, bf16[16,256]{1,0:T(8,128)(2,1)} %slice.17.ending), custom_call_target="tpu_custom_call" | custom-call | tf_op jit(solution)/shard_map/attend/pallas_call | solution.py:239
  86.0 10.2 %all-to-all-start.1 = ((bf16[8,272,256]{2,1,0:T(8,128)(2,1)}), bf16[8,272,256]{2,1,0:T(8,128)(2,1)S(1)}, u32[]{:S(2)}, u32[]{:S(2)}) async-start(bf16[8,272,256]{2,1,0:T(8,128)(2,1)} %attend.1), calls=%async_computation.1 | async-start | bytes 2228224 | tf_op jit(solution)/shard_map/all_to_all | solution.py:316
  96.9 3.8 %gates.1 = (bf16[256,128]{1,0:T(8,128)(2,1)}, bf16[256,128]{1,0:T(8,128)(2,1)}, bf16[256,128]{1,0:T(8,128)(2,1)}) custom-call(bf16[256,2048]{1,0:T(8,128)(2,1)} %get-tuple-element.17.normed, f32[256,128]{1,0:T(8,128)} %get-tuple-element.18.scale, bf16[2048,128]{1,0:T(8,128)(2,1)} %gw.1, bf16[2048,128]{1,0:T(8,128)(2,1)} %ow.1, bf16[2048,128]{1,0:T(8,128)(2,1)} %iw.3, ...), custom_call_target="tpu_custom_call" | custom-call | flops 536870912 | bytes 2097152 | tf_op jit(solution)/shard_map/gates/pallas_call | solution.py:220
  100.7 6.0 %all-to-all-done.1.parts = bf16[8,272,256]{2,1,0:T(8,128)(2,1)S(1)} async-done(((bf16[8,272,256]{2,1,0:T(8,128)(2,1)}), bf16[8,272,256]{2,1,0:T(8,128)(2,1)S(1)}, u32[]{:S(2)}, u32[]{:S(2)}) %all-to-all-start.1) | async-done | bytes 1114144 | tf_op jit(solution)/shard_map/all_to_all | solution.py:316
  106.7 0.0 copy-start
  106.7 1.0 copy-done
  107.7 4.4 %finish.1 = (bf16[256,2048]{1,0:T(8,128)(2,1)}, f32[1,2,256]{2,1,0:T(2,128)}) custom-call(f32[1]{0:T(128)S(6)} %copy.16.lam, bf16[8,272,256]{2,1,0:T(8,128)(2,1)} %copy-done, bf16[256,128]{1,0:T(8,128)(2,1)} %get-tuple-element.19.gate, bf16[256,128]{1,0:T(8,128)(2,1)} %get-tuple-element.20.outer, bf16[256,128]{1,0:T(8,128)(2,1)} %get-tuple-element.21.insig, ...), custom_call_target="tpu_custom_call" | custom-call | tf_op jit(solution)/shard_map/finish/pallas_call | solution.py:252
  112.0 20.0 %all_to_all.15 = bf16[8,32,2048]{2,1,0:T(8,128)(2,1)S(1)} all-to-all(bf16[8,32,2048]{2,1,0:T(8,128)(2,1)} %bitcast.8), channel_id=1, replica_groups=mesh['sp'=64,'tp'=8] {'tp'}, dimensions={0} | all-to-all | bytes 2097152 | tf_op jit(solution)/shard_map/all_to_all | solution.py:320
  132.1 0.8 reduce_sum.12
  (3 shorter events, 0.0 us)
Async XLA Ops:
  14.0 3.8 %copy-start.1 = (bf16[1024,256]{1,0:T(8,128)(2,1)}, bf16[1024,256]{1,0:T(8,128)(2,1)S(1)}, u32[]{:S(2)}) copy-start(bf16[1024,256]{1,0:T(8,128)(2,1)S(1)} %all-gather) | copy-start | bytes 1572868
  14.0 3.8 %collective-permute-start = (bf16[4,256,256]{2,1,0:T(8,128)(2,1)S(1)}, bf16[4,256,256]{2,1,0:T(8,128)(2,1)S(1)}, u32[]{:S(2)}, u32[]{:S(2)}) collective-permute-start(bf16[4,256,256]{2,1,0:T(8,128)(2,1)S(1)} %bitcast.6), channel_id=1, source_target_pairs={{0,1},{1,0},{2,3},{3,2},{4,5},{5,4},{6,7},{7,6},{8,9},{9,8},{10,11... | collective-permute-start | bytes 1572872 | tf_op jit(solution)/shard_map/ppermute | solution.py:301
  17.8 0.8 copy-start.4
  23.1 6.1 %copy-start.3 = (bf16[272,256]{1,0:T(8,128)(2,1)S(1)}, bf16[272,256]{1,0:T(8,128)(2,1)}, u32[]{:S(2)}) copy-start(bf16[272,256]{1,0:T(8,128)(2,1)} %get-tuple-element.15.own) | copy-start | bytes 417796
  23.1 48.9 %all-to-all-start = ((bf16[8,256,128]{2,1,0:T(8,128)(2,1)}), bf16[8,256,128]{2,1,0:T(8,128)(2,1)S(1)}, u32[]{:S(2)}, u32[]{:S(2)}) async-start(bf16[8,256,128]{2,1,0:T(8,128)(2,1)} %get-tuple-element.14), calls=%async_computation | async-start | bytes 1048576 | tf_op jit(solution)/shard_map/all_to_all | solution.py:311
  29.1 8.0 %collective-permute-start.1 = (bf16[240,256]{1,0:T(8,128)(2,1)S(1)}, bf16[240,256]{1,0:T(8,128)(2,1)S(1)}, u32[]{:S(2)}, u32[]{:S(2)}) collective-permute-start(bf16[240,256]{1,0:T(8,128)(2,1)S(1)} %slice.12), channel_id=1, source_target_pairs={{0,64},{8,72},{16,80},{24,88},{32,96},{40,104},{48,112},{56,120},{... | collective-permute-start | bytes 368648 | tf_op jit(solution)/shard_map/ppermute | solution.py:270
  72.0 0.8 copy-start.2
  86.0 20.6 %all-to-all-start.1 = ((bf16[8,272,256]{2,1,0:T(8,128)(2,1)}), bf16[8,272,256]{2,1,0:T(8,128)(2,1)S(1)}, u32[]{:S(2)}, u32[]{:S(2)}) async-start(bf16[8,272,256]{2,1,0:T(8,128)(2,1)} %attend.1), calls=%async_computation.1 | async-start | bytes 2228224 | tf_op jit(solution)/shard_map/all_to_all | solution.py:316
  106.7 1.0 copy-start

commit v5 on v4

--- a/solution.py
+++ b/solution.py
@@ -13,15 +13,16 @@
 HIDDEN = -1e30
 
 
-def project_kernel(own, other, gain, qw, kw, vw, iw, sw, kv, q, normed, scaled):
+def project_kernel(own, gain, qw, kw, vw, iw, sw, other, kv, shifted, q, normed, scaled):
     count, rows, part = own.shape
     width = normed.shape[1]
-    tail = kv.shape[0] - rows
+    skipped = rows // q.shape[0]
+    tail = shifted.shape[0] + skipped - rows
 
     def spread(core):
         squares = jnp.zeros((rows, part), jnp.float32)
-        for x in range(count):
-            for ref, side in ((own, core), (other, 1 - core)):
+        for ref, side in ((own, core), (other, 1 - core)):
+            for x in range(count):
                 at = (2 * x + side) * part
                 piece = ref[x].astype(jnp.float32)
                 squares = squares + piece * piece
@@ -36,12 +37,15 @@
             return raw.astype(jnp.bfloat16)
 
         columns = kw.shape[1]
-        kv[:rows, :columns] = project(kw)
-        kv[:rows, columns:] = project(vw)
+        for n, weight in enumerate((kw, vw)):
+            cut = slice(n * columns, (n + 1) * columns)
+            values = project(weight)
+            kv[:, cut] = values
+            shifted[: rows - skipped, cut] = values[skipped:]
         low = rows - tail
         ending = project(iw, low).astype(jnp.float32) * project(sw, low).astype(jnp.float32)
-        kv[rows:, :columns] = ending.astype(jnp.bfloat16)
-        kv[rows:, columns:] = jnp.zeros((tail, columns), jnp.bfloat16)
+        shifted[rows - skipped :, :columns] = ending.astype(jnp.bfloat16)
+        shifted[rows - skipped :, columns:] = jnp.zeros((tail, columns), jnp.bfloat16)
         query = project(qw, 0, LOG2E * (columns // 2) ** -0.5)
         for i in range(q.shape[0]):
             q[i] = query
@@ -61,7 +65,7 @@
     gate[...] = project(gw)
 
 
-def attend_kernel(chunk, span, q, own, kv, ending, out, held):
+def attend_kernel(chunk, span, q, own, ending, moved, kv, out, held):
     rows = q.shape[1]
     columns = kv.shape[2]
     value_size = columns // 2
@@ -80,7 +84,7 @@
         col = lax.broadcasted_iota(jnp.int32, (rows, rows), 1)
 
         def part(b, cut):
-            return own[:rows, cut] if b is None else kv[b, :, cut]
+            return own[:, cut] if b is None else kv[b, :, cut]
 
         def seen(i):
             return row + (first + i - slot) * rows >= col
@@ -89,7 +93,7 @@
             i, m = units[u]
             cut = slice(m * key_size, (m + 1) * key_size)
             s = lax.dot_general(
-                q[i, :, cut], part(b, cut), (((1,), (1,)), ((), ())), preferred_element_type=jnp.float32
+                q[first + i, :, cut], part(b, cut), (((1,), (1,)), ((), ())), preferred_element_type=jnp.float32
             )
             if b is None:
                 s = jnp.where(seen(i), s, HIDDEN)
@@ -137,7 +141,8 @@
                     rest = rest - rounded
             tail = out.shape[1] - rows
             turned = jnp.transpose(spread)[:tail].astype(jnp.bfloat16)
-            ends = jnp.concatenate([own[rows:, :value_size], ending[:, :value_size]], axis=1)
+            ends = [ref[ref.shape[0] - tail :, :value_size] for ref in (ending, moved)]
+            ends = jnp.concatenate(ends, axis=1)
             line = lax.broadcasted_iota(jnp.int32, (tail, columns), 0)
             out[i, rows:, :] = jnp.where(line < tail // 2, turned, ends)
 
@@ -145,10 +150,11 @@
         pl.when(last == full)(functools.partial(body, full))
 
 
-def finish_kernel(lam, parts, gate, outer, insig, taps, head_gain, attn_w, conv_w, mixed, totals):
+def finish_kernel(lam, gate, outer, insig, taps, head_gain, attn_w, conv_w, parts, mixed, totals):
     count, _, columns = parts.shape
     rows = gate.shape[0]
     value_size = columns // 2
+
     tails = [parts[j, rows:, :].astype(jnp.float32) for j in range(count)]
     logs = [t[0:2] + t[2:4] + t[4:6] for t in tails]
     top = logs[0]
@@ -162,17 +168,6 @@
     shares = [share / total for share in shares]
     pad = jnp.zeros((value_size - 2 * count, rows), jnp.float32)
     turned = jnp.transpose(jnp.concatenate([*shares, pad], axis=0))
-    mapped = []
-    for m in range(2):
-        summed = jnp.zeros((rows, value_size), jnp.float32)
-        for j in range(count):
-            piece = parts[j, :rows, m * value_size : (m + 1) * value_size].astype(jnp.float32)
-            summed = summed + turned[:, 2 * j + m : 2 * j + m + 1] * piece
-        mapped.append(summed)
-    diff = mapped[0] - lam[0] * mapped[1]
-    norm = lax.rsqrt(jnp.mean(diff * diff, axis=-1, keepdims=True) + 1e-05)
-    opened = gate[...].astype(jnp.float32)
-    head = diff * norm * head_gain[...] * (opened / (1.0 + jnp.exp(-opened)))
     slot = lax.rem(lax.axis_index("sp"), count)
     ends = parts[lax.rem(slot + count - 1, count), rows:, :].astype(jnp.float32)
     ends = jnp.where(slot == 0, ends[:, value_size:], ends[:, :value_size])
@@ -187,6 +182,15 @@
             moved = jnp.where(row == at, ends[line : line + 1, :], moved)
         convolved = convolved + taps[reach - by : reach - by + 1, :] * moved
     conv = (outer[...].astype(jnp.float32) * convolved).astype(jnp.bfloat16)
+    mapped = [jnp.zeros((rows, value_size), jnp.float32) for _ in range(2)]
+    for j in range(count):
+        for m in range(2):
+            piece = parts[j, :rows, m * value_size : (m + 1) * value_size].astype(jnp.float32)
+            mapped[m] = mapped[m] + turned[:, 2 * j + m : 2 * j + m + 1] * piece
+    diff = mapped[0] - lam[0] * mapped[1]
+    norm = lax.rsqrt(jnp.mean(diff * diff, axis=-1, keepdims=True) + 1e-05)
+    opened = gate[...].astype(jnp.float32)
+    head = diff * norm * head_gain[...] * (opened / (1.0 + jnp.exp(-opened)))
     mixed[...] = (
         jnp.dot(head.astype(jnp.bfloat16), attn_w[...], preferred_element_type=jnp.float32)
         + jnp.dot(conv, conv_w[...], preferred_element_type=jnp.float32)
@@ -195,6 +199,10 @@
 
 VMEM = pl.BlockSpec(memory_space=pltpu.VMEM)
 SMEM = pl.BlockSpec(memory_space=pltpu.SMEM)
+
+
+def close(array):
+    return pltpu.with_memory_space_constraint(array, pltpu.VMEM)
 
 
 def project(own, other, gain, weights, copies, tail):
@@ -204,15 +212,16 @@
     return pl.pallas_call(
         project_kernel,
         out_shape=(
-            jax.ShapeDtypeStruct((rows + tail, 2 * columns), jnp.bfloat16),
-            jax.ShapeDtypeStruct((copies, rows, columns), jnp.bfloat16),
+            pltpu.VMEM((rows, 2 * columns), jnp.bfloat16),
+            pltpu.VMEM((rows - rows // copies + tail, 2 * columns), jnp.bfloat16),
+            pltpu.VMEM((copies, rows, columns), jnp.bfloat16),
             jax.ShapeDtypeStruct((rows, width), jnp.bfloat16),
             jax.ShapeDtypeStruct((rows, columns), jnp.float32),
         ),
         in_specs=[VMEM] * 8,
-        out_specs=(VMEM,) * 4,
+        out_specs=(VMEM,) * 5,
         name="project",
-    )(own, other, gain.reshape(1, width), *weights)
+    )(close(own), gain.reshape(1, width), *weights, close(other))
 
 
 def gates(normed, scale, weights):
@@ -227,10 +236,9 @@
     )(normed, scale, *weights)
 
 
-def attend(queries, own, kv, ending, chunk):
-    count, rows, columns = queries.shape
+def attend(queries, own, ending, moved, kv, chunk, extra):
+    count, rows, _ = queries.shape
     others, _, wide = kv.shape
-    extra = ending.shape[0]
     span = 2
 
     def tiled(length, width):
@@ -240,38 +248,38 @@
         functools.partial(attend_kernel, chunk, span),
         grid=(count // span,),
         out_shape=jax.ShapeDtypeStruct((count, rows + extra, wide), jnp.bfloat16),
-        in_specs=[tiled(rows, columns), VMEM, VMEM, VMEM],
+        in_specs=[VMEM] * 5,
         out_specs=tiled(rows + extra, wide),
         scratch_shapes=[pltpu.VMEM((2, others + 1, rows, rows), jnp.float32)],
         name="attend",
-    )(queries, own, kv, ending)
-
-
-def finish(lambdas, parts, gate, outer, insig, taps, head_gain, attn_w, conv_w):
+    )(close(queries), close(own), close(ending), close(moved), close(kv))
+
+
+def finish(parts, lambdas, gate, outer, insig, taps, head_gain, attn_w, conv_w):
     rows = gate.shape[0]
     return pl.pallas_call(
         finish_kernel,
         out_shape=(
-            jax.ShapeDtypeStruct((rows, attn_w.shape[1]), jnp.bfloat16),
+            pltpu.VMEM((rows, attn_w.shape[1]), jnp.bfloat16),
             jax.ShapeDtypeStruct((1, 2, rows), jnp.float32),
         ),
         in_specs=[SMEM] + [VMEM] * 8,
         out_specs=(VMEM, VMEM),
         name="finish",
-    )(lambdas, parts, gate, outer, insig, taps, head_gain.reshape(1, -1), attn_w, conv_w)
-
-
-def earlier_blocks(block, groups, chunk, tail):
+    )(lambdas, gate, outer, insig, taps, head_gain.reshape(1, -1), attn_w, conv_w, close(parts))
+
+
+def earlier_blocks(block, shifted, groups, chunk):
     devices = lax.axis_size("sp")
     count = devices // chunk
-    rows, wide = block.shape[0] - tail, block.shape[1]
+    rows, wide = block.shape
     step = rows // count
     share = rows - step
-    before = lax.ppermute(block[step:], "sp", [(i, i + chunk) for i in range(devices - chunk)])
+    moved = lax.ppermute(shifted, "sp", [(i, i + chunk) for i in range(devices - chunk)])
     start = share - lax.div(lax.axis_index("sp"), chunk) * step
-    held = lax.dynamic_slice_in_dim(jnp.concatenate([before[:share], block[:rows]], axis=0), start, share, 0)
+    held = lax.dynamic_slice_in_dim(jnp.concatenate([moved[:share], block], axis=0), start, share, 0)
     gathered = lax.all_gather(held, "sp", axis_index_groups=groups, tiled=True)
-    return gathered.reshape(count - 1, rows, wide), before[share:]
+    return gathered.reshape(count - 1, rows, wide), moved
 
 
 def per_device(
@@ -300,7 +308,7 @@
     own = lax.all_gather(tokens, "tp", axis_index_groups=same_core)
     other = lax.ppermute(own, "tp", [(i, i ^ 1) for i in range(tp)])
     tail = 16
-    kv, query, normed, scale = project(
+    kv, shifted, query, normed, scale = project(
         own,
         other,
         norm_gain,
@@ -309,13 +317,13 @@
         tail,
     )
     queries = lax.all_to_all(query, "sp", 0, 0, axis_index_groups=near, tiled=True)
-    earlier, ending = earlier_blocks(kv, far, chunk, tail)
-    parts = attend(queries, kv, earlier, ending, chunk)
+    earlier, moved = earlier_blocks(kv, shifted, far, chunk)
+    parts = attend(queries, kv, shifted, moved, earlier, chunk, tail)
     normed, parts = lax.optimization_barrier((normed, parts))
     gate, outer, insig = gates(normed, scale, (gate_weight, outer_weight, inner_weight, signal_weight))
     parts = lax.all_to_all(parts, "sp", 0, 0, axis_index_groups=near, tiled=True)
     partial, log_totals = finish(
-        lambdas, parts, gate, outer, insig, conv_taps, head_gain, attn_out_weight, conv_out_weight
+        parts, lambdas, gate, outer, insig, conv_taps, head_gain, attn_out_weight, conv_out_weight
     )
     tiles = lax.all_to_all(partial.reshape(tp, -1, partial.shape[1]), "tp", 0, 0, tiled=True)
     mixed = jnp.sum(tiles.astype(jnp.float32), axis=0).astype(jnp.bfloat16)

time: 134 us -> 126 us (0.940)
  local copies, waits for them, and re-layouts: 3.22 us -> 0.01 us
  blocking collectives: 67.4 us -> 64.5 us
  Pallas kernels: 25.9 us -> 23.5 us
    unnamed x10 -> x0, local copies, waits for them, and re-layouts: 2.6 us -> none
    all_gather x1, blocking collectives: 34 us -> 32 us  [earlier_blocks(): gathered = lax.all_gather(held, 'sp', axis_index_groups=groups, tiled=True)]
  transfers between devices with their start and end apart: 4 -> 4, of which waited for: 3 -> 3; matrix products, arithmetic and copies ran while one was open for 1% -> 0% of each run, Pallas kernels for 3% -> 3%
where the time goes in v5:
time: 126 us; the launch traced here: 125 us
  blocking collectives  64.5 us (51%)
  Pallas kernels  23.5 us (19%)
  starting transfers between devices  20.3 us (16%)
  waiting for transfers between devices  14.5 us (12%)
  between operations  1.33 us (1%)
    all_gather x1, blocking collectives, earlier_blocks(): gathered = lax.all_gather(held, 'sp', axis_index_groups=groups, tiled=True)  32 us
    all_to_all x1, blocking collectives, per_device(): lax.all_to_all(partial.reshape(tp, -1, partial.shape[1]), 'tp', 0, 0, til...  19.1 us
    all_gather x1, blocking collectives, per_device(): own = lax.all_gather(tokens, 'tp', axis_index_groups=same_core)  13.3 us
    pallas_call x1, Pallas kernels, attend(): pl.pallas_call(functools.partial(attend_kernel, chunk, span), grid=(count...  12.1 us
    all_to_all x1, starting transfers between devices, per_device(): lax.all_to_all(parts, 'sp', 0, 0, axis_index_groups=near, tiled=True)  11.2 us
    ppermute x1, waiting for transfers between devices, earlier_blocks(): lax.ppermute(shifted, 'sp', [(i, i + chunk) for i in range(devices - chun...  6.65 us
    all_to_all x1, waiting for transfers between devices, per_device(): lax.all_to_all(parts, 'sp', 0, 0, axis_index_groups=near, tiled=True)  5.95 us
    all_to_all x1, starting transfers between devices, per_device(): lax.all_to_all(query, 'sp', 0, 0, axis_index_groups=near, tiled=True)  5.92 us
  transfers between devices with their start and end apart: 4, of which 3 were waited for; matrix products, arithmetic and copies ran while one was open for 0% of the time, Pallas kernels for 3%

profile of v5, /device:TPU:480, one launch (start us, length us, event | category | flops | bytes accessed | tf_op | source)
XLA Modules:
  0.0 125.2 jit_solution(14622569694339265349)
XLA Ops:
  0.6 13.3 %all-gather = bf16[1024,256]{1,0:T(8,128)(2,1)S(1)} all-gather(bf16[256,256]{1,0:T(8,128)(2,1)} %param.14), channel_id=2, replica_groups={{0,2,4,6},{1,3,5,7},{8,10,12,14},{9,11,13,15},{16,18,20,22},{17,19,21,2..., dimensions={0}, use_global_device_ids=true | all-gather | bytes 655360 | tf_op jit(solution)/shard_map/all_gather | solution.py:308
  14.0 1.9 %collective-permute-start = (bf16[4,256,256]{2,1,0:T(8,128)(2,1)S(1)}, bf16[4,256,256]{2,1,0:T(8,128)(2,1)S(1)}, u32[]{:S(2)}, u32[]{:S(2)}) collective-permute-start(bf16[4,256,256]{2,1,0:T(8,128)(2,1)S(1)} %bitcast.6), channel_id=1, source_target_pairs={{0,1},{1,0},{2,3},{3,2},{4,5},{5,4},{6,7},{7,6},{8,9},{9,8},{10,11... | collective-permute-start | bytes 1572872 | tf_op jit(solution)/shard_map/ppermute | solution.py:309
  15.9 1.9 %collective-permute-done.other = bf16[4,256,256]{2,1,0:T(8,128)(2,1)S(1)} collective-permute-done((bf16[4,256,256]{2,1,0:T(8,128)(2,1)S(1)}, bf16[4,256,256]{2,1,0:T(8,128)(2,1)S(1)}, u32[]{:S(2)}, u32[]{:S(2)}) %collective-permute-start) | collective-permute-done | bytes 524320 | tf_op jit(solution)/shard_map/ppermute | solution.py:309
  17.8 4.2 %project.1 = (bf16[256,256]{1,0:T(8,128)(2,1)S(1)}, bf16[240,256]{1,0:T(8,128)(2,1)S(1)}, bf16[8,256,128]{2,1,0:T(8,128)(2,1)}, bf16[256,2048]{1,0:T(8,128)(2,1)}, f32[256,128]{1,0:T(8,128)}) custom-call(bf16[4,256,256]{2,1,0:T(8,128)(2,1)S(1)} %bitcast.7, f32[1,2048]{1,0:T(1,128)} %bitcast.9, bf16[2048,128]{1,0:T(8,128)(2,1)} %qw.1, bf16[2048,128]{1,0:T(8,128)(2,1)} %kw.1, ...), custom_call_target="tpu_custom_call" | custom-call | tf_op jit(solution)/shard_map/project/pallas_call | solution.py:212
  21.9 5.9 %all-to-all-start = ((bf16[8,256,128]{2,1,0:T(8,128)(2,1)}), bf16[8,256,128]{2,1,0:T(8,128)(2,1)S(1)}, u32[]{:S(2)}, u32[]{:S(2)}) async-start(bf16[8,256,128]{2,1,0:T(8,128)(2,1)} %get-tuple-element.15), calls=%async_computation | async-start | bytes 1048576 | tf_op jit(solution)/shard_map/all_to_all | solution.py:319
  27.9 1.3 %collective-permute-start.1 = (bf16[240,256]{1,0:T(8,128)(2,1)S(1)}, bf16[240,256]{1,0:T(8,128)(2,1)S(1)}, u32[]{:S(2)}, u32[]{:S(2)}) collective-permute-start(bf16[240,256]{1,0:T(8,128)(2,1)S(1)} %get-tuple-element.17.ending), channel_id=1, source_target_pairs={{0,64},{8,72},{16,80},{24,88},{32,96},{40,104},{48,112},{56,120},{... | collective-permute-start | bytes 368648 | tf_op jit(solution)/shard_map/ppermute | solution.py:278
  29.2 6.7 %collective-permute-done.1.moved = bf16[240,256]{1,0:T(8,128)(2,1)S(1)} collective-permute-done((bf16[240,256]{1,0:T(8,128)(2,1)S(1)}, bf16[240,256]{1,0:T(8,128)(2,1)S(1)}, u32[]{:S(2)}, u32[]{:S(2)}) %collective-permute-start.1) | collective-permute-done | bytes 122912 | tf_op jit(solution)/shard_map/ppermute | solution.py:278
  35.8 0.3 fusion
  36.1 32.0 %all_gather.11 = bf16[1792,256]{1,0:T(8,128)(2,1)S(1)} all-gather(bf16[224,256]{1,0:T(8,128)(2,1)S(1)} %fusion), channel_id=1, replica_groups={{0,64,128,192,256,320,384,448},{8,72,136,200,264,328,392,456},{16,80,14..., dimensions={0}, use_global_device_ids=true | all-gather | bytes 1032192 | tf_op jit(solution)/shard_map/all_gather | solution.py:281
  68.1 0.0 all-to-all-done.q
  68.1 12.1 %attend.1 = bf16[8,272,256]{2,1,0:T(8,128)(2,1)} custom-call(bf16[8,256,128]{2,1,0:T(8,128)(2,1)S(1)} %all-to-all-done.q, bf16[256,256]{1,0:T(8,128)(2,1)S(1)} %get-tuple-element.16.own, bf16[240,256]{1,0:T(8,128)(2,1)S(1)} %get-tuple-element.17.ending, bf16[240,256]{1,0:T(8,128)(2,1)S(1)} %collective-permute-done.1.moved, bf16[7,256,256]{2,1,0:T(8,128)(2,1)S(1)} %bitcast.5), custom_call_target="tpu_custom_call" | custom-call | tf_op jit(solution)/shard_map/attend/pallas_call | solution.py:247
  80.2 11.2 %all-to-all-start.1 = ((bf16[8,272,256]{2,1,0:T(8,128)(2,1)}), bf16[8,272,256]{2,1,0:T(8,128)(2,1)S(1)}, u32[]{:S(2)}, u32[]{:S(2)}) async-start(bf16[8,272,256]{2,1,0:T(8,128)(2,1)} %attend.1), calls=%async_computation.1 | async-start | bytes 2228224 | tf_op jit(solution)/shard_map/all_to_all | solution.py:324
  92.0 3.8 %gates.1 = (bf16[256,128]{1,0:T(8,128)(2,1)}, bf16[256,128]{1,0:T(8,128)(2,1)}, bf16[256,128]{1,0:T(8,128)(2,1)}) custom-call(bf16[256,2048]{1,0:T(8,128)(2,1)} %get-tuple-element.18.normed, f32[256,128]{1,0:T(8,128)} %get-tuple-element.19.scale, bf16[2048,128]{1,0:T(8,128)(2,1)} %gw.1, bf16[2048,128]{1,0:T(8,128)(2,1)} %ow.1, bf16[2048,128]{1,0:T(8,128)(2,1)} %iw.3, ...), custom_call_target="tpu_custom_call" | custom-call | flops 536870912 | bytes 2097152 | tf_op jit(solution)/shard_map/gates/pallas_call | solution.py:229
  95.8 5.9 %all-to-all-done.1.parts = bf16[8,272,256]{2,1,0:T(8,128)(2,1)S(1)} async-done(((bf16[8,272,256]{2,1,0:T(8,128)(2,1)}), bf16[8,272,256]{2,1,0:T(8,128)(2,1)S(1)}, u32[]{:S(2)}, u32[]{:S(2)}) %all-to-all-start.1) | async-done | bytes 1114144 | tf_op jit(solution)/shard_map/all_to_all | solution.py:324
  101.8 3.5 %finish.1 = (bf16[256,2048]{1,0:T(8,128)(2,1)S(1)}, f32[1,2,256]{2,1,0:T(2,128)}) custom-call(f32[1]{0:T(128)S(6)} %copy.16.lam, bf16[256,128]{1,0:T(8,128)(2,1)} %get-tuple-element.20.gate, bf16[256,128]{1,0:T(8,128)(2,1)} %get-tuple-element.21.outer, bf16[256,128]{1,0:T(8,128)(2,1)} %get-tuple-element.22.insig, f32[3,128]{1,0:T(4,128)} %taps.1, ...), custom_call_target="tpu_custom_call" | custom-call | tf_op jit(solution)/shard_map/finish/pallas_call | solution.py:260
  105.2 19.1 %all_to_all.15 = bf16[8,32,2048]{2,1,0:T(8,128)(2,1)S(1)} all-to-all(bf16[8,32,2048]{2,1,0:T(8,128)(2,1)S(1)} %bitcast.8), channel_id=1, replica_groups=mesh['sp'=64,'tp'=8] {'tp'}, dimensions={0} | all-to-all | bytes 2097152 | tf_op jit(solution)/shard_map/all_to_all | solution.py:328
  124.4 0.8 reduce_sum.12
  (1 shorter events, 0.0 us)
Async XLA Ops:
  14.0 3.8 %collective-permute-start = (bf16[4,256,256]{2,1,0:T(8,128)(2,1)S(1)}, bf16[4,256,256]{2,1,0:T(8,128)(2,1)S(1)}, u32[]{:S(2)}, u32[]{:S(2)}) collective-permute-start(bf16[4,256,256]{2,1,0:T(8,128)(2,1)S(1)} %bitcast.6), channel_id=1, source_target_pairs={{0,1},{1,0},{2,3},{3,2},{4,5},{5,4},{6,7},{7,6},{8,9},{9,8},{10,11... | collective-permute-start | bytes 1572872 | tf_op jit(solution)/shard_map/ppermute | solution.py:309
  21.9 46.2 %all-to-all-start = ((bf16[8,256,128]{2,1,0:T(8,128)(2,1)}), bf16[8,256,128]{2,1,0:T(8,128)(2,1)S(1)}, u32[]{:S(2)}, u32[]{:S(2)}) async-start(bf16[8,256,128]{2,1,0:T(8,128)(2,1)} %get-tuple-element.15), calls=%async_computation | async-start | bytes 1048576 | tf_op jit(solution)/shard_map/all_to_all | solution.py:319
  27.9 7.9 %collective-permute-start.1 = (bf16[240,256]{1,0:T(8,128)(2,1)S(1)}, bf16[240,256]{1,0:T(8,128)(2,1)S(1)}, u32[]{:S(2)}, u32[]{:S(2)}) collective-permute-start(bf16[240,256]{1,0:T(8,128)(2,1)S(1)} %get-tuple-element.17.ending), channel_id=1, source_target_pairs={{0,64},{8,72},{16,80},{24,88},{32,96},{40,104},{48,112},{56,120},{... | collective-permute-start | bytes 368648 | tf_op jit(solution)/shard_map/ppermute | solution.py:278
  80.2 21.5 %all-to-all-start.1 = ((bf16[8,272,256]{2,1,0:T(8,128)(2,1)}), bf16[8,272,256]{2,1,0:T(8,128)(2,1)S(1)}, u32[]{:S(2)}, u32[]{:S(2)}) async-start(bf16[8,272,256]{2,1,0:T(8,128)(2,1)} %attend.1), calls=%async_computation.1 | async-start | bytes 2228224 | tf_op jit(solution)/shard_map/all_to_all | solution.py:324

commit v6 on v5

--- a/solution.py
+++ b/solution.py
@@ -150,7 +150,7 @@
         pl.when(last == full)(functools.partial(body, full))
 
 
-def finish_kernel(lam, gate, outer, insig, taps, head_gain, attn_w, conv_w, parts, mixed, totals):
+def finish_kernel(group, lam, gate, outer, insig, taps, head_gain, attn_w, conv_w, parts, theirs, kept, totals):
     count, _, columns = parts.shape
     rows = gate.shape[0]
     value_size = columns // 2
@@ -191,9 +191,29 @@
     norm = lax.rsqrt(jnp.mean(diff * diff, axis=-1, keepdims=True) + 1e-05)
     opened = gate[...].astype(jnp.float32)
     head = diff * norm * head_gain[...] * (opened / (1.0 + jnp.exp(-opened)))
-    mixed[...] = (
-        jnp.dot(head.astype(jnp.bfloat16), attn_w[...], preferred_element_type=jnp.float32)
-        + jnp.dot(conv, conv_w[...], preferred_element_type=jnp.float32)
+    side = lax.rem(lax.axis_index("tp"), 2)
+    share = theirs.shape[0] // group
+    halves = [
+        jnp.reshape(part, (group, 2, share, part.shape[1])) for part in (head.astype(jnp.bfloat16), conv)
+    ]
+
+    def chosen(half, core):
+        return jnp.where(core == 0, half[:, 0], half[:, 1]).reshape(group * share, half.shape[3])
+
+    theirs[...] = (
+        jnp.dot(chosen(halves[0], 1 - side), attn_w[...], preferred_element_type=jnp.float32)
+        + jnp.dot(chosen(halves[1], 1 - side), conv_w[...], preferred_element_type=jnp.float32)
+    ).astype(jnp.bfloat16)
+    kept[:, :value_size] = chosen(halves[0], side)
+    kept[:, value_size:] = chosen(halves[1], side)
+
+
+def join_kernel(kept, received, attn_w, conv_w, out):
+    size = attn_w.shape[0]
+    out[...] = (
+        jnp.dot(kept[:, :size], attn_w[...], preferred_element_type=jnp.float32)
+        + jnp.dot(kept[:, size:], conv_w[...], preferred_element_type=jnp.float32)
+        + received[...].astype(jnp.float32)
     ).astype(jnp.bfloat16)
 
 
@@ -255,18 +275,29 @@
     )(close(queries), close(own), close(ending), close(moved), close(kv))
 
 
-def finish(parts, lambdas, gate, outer, insig, taps, head_gain, attn_w, conv_w):
-    rows = gate.shape[0]
-    return pl.pallas_call(
-        finish_kernel,
+def finish(group, parts, lambdas, gate, outer, insig, taps, head_gain, attn_w, conv_w):
+    rows, size = gate.shape
+    return pl.pallas_call(
+        functools.partial(finish_kernel, group),
         out_shape=(
-            pltpu.VMEM((rows, attn_w.shape[1]), jnp.bfloat16),
+            pltpu.VMEM((rows // 2, attn_w.shape[1]), jnp.bfloat16),
+            pltpu.VMEM((rows // 2, 2 * size), jnp.bfloat16),
             jax.ShapeDtypeStruct((1, 2, rows), jnp.float32),
         ),
         in_specs=[SMEM] + [VMEM] * 8,
-        out_specs=(VMEM, VMEM),
+        out_specs=(VMEM, VMEM, VMEM),
         name="finish",
     )(lambdas, gate, outer, insig, taps, head_gain.reshape(1, -1), attn_w, conv_w, close(parts))
+
+
+def join(kept, received, attn_w, conv_w):
+    return pl.pallas_call(
+        join_kernel,
+        out_shape=pltpu.VMEM(received.shape, jnp.bfloat16),
+        in_specs=[VMEM] * 4,
+        out_specs=VMEM,
+        name="join",
+    )(close(kept), close(received), attn_w, conv_w)
 
 
 def earlier_blocks(block, shifted, groups, chunk):
@@ -322,10 +353,14 @@
     normed, parts = lax.optimization_barrier((normed, parts))
     gate, outer, insig = gates(normed, scale, (gate_weight, outer_weight, inner_weight, signal_weight))
     parts = lax.all_to_all(parts, "sp", 0, 0, axis_index_groups=near, tiled=True)
-    partial, log_totals = finish(
-        parts, lambdas, gate, outer, insig, conv_taps, head_gain, attn_out_weight, conv_out_weight
-    )
-    tiles = lax.all_to_all(partial.reshape(tp, -1, partial.shape[1]), "tp", 0, 0, tiled=True)
+    theirs, kept, log_totals = finish(
+        tp // 2, parts, lambdas, gate, outer, insig, conv_taps, head_gain, attn_out_weight, conv_out_weight
+    )
+    received = lax.ppermute(theirs, "tp", [(i, i ^ 1) for i in range(tp)])
+    partial = join(kept, received, attn_out_weight, conv_out_weight)
+    tiles = lax.all_to_all(
+        partial.reshape(tp // 2, -1, partial.shape[1]), "tp", 0, 0, axis_index_groups=same_core, tiled=True
+    )
     mixed = jnp.sum(tiles.astype(jnp.float32), axis=0).astype(jnp.bfloat16)
     return mixed, log_totals
 

time: 126 us -> 124 us (0.984)
  blocking collectives: 64.5 us -> 58.3 us
  starting transfers between devices: 20.3 us -> 22.2 us
  waiting for transfers between devices: 14.5 us -> 16.4 us
    all_to_all x1, blocking collectives: 19.1 us -> 12.9 us  [per_device(): lax.all_to_all(partial.reshape(tp // 2, -1, partial.shape[1]), 'tp', 0, 0...]
    ppermute x0 -> x1, starting transfers between devices: none -> 1.91 us  [per_device(): received = lax.ppermute(theirs, 'tp', [(i, i ^ 1) for i in range(tp)])]
    ppermute x0 -> x1, waiting for transfers between devices: none -> 1.88 us  [per_device(): received = lax.ppermute(theirs, 'tp', [(i, i ^ 1) for i in range(tp)])]
    pallas_call x1 -> x2, Pallas kernels: 3.47 us -> 4.63 us  [the longest x1 3.01 us: finish(): pl.pallas_call(functools.partial(finish_kernel, group), out_shape=(pltpu....]
  transfers between devices with their start and end apart: 4 -> 5, of which waited for: 3 -> 4; matrix products, arithmetic and copies ran while one was open for 0% -> 0% of each run, Pallas kernels for 3% -> 3%
where the time goes in v6:
time: 124 us
  blocking collectives  58.3 us (47%)
  Pallas kernels  24.7 us (20%)
  starting transfers between devices  22.2 us (18%)
  waiting for transfers between devices  16.4 us (13%)
  between operations  1.34 us (1%)
    all_gather x1, blocking collectives, earlier_blocks(): gathered = lax.all_gather(held, 'sp', axis_index_groups=groups, tiled=True)  32 us
    all_gather x1, blocking collectives, per_device(): own = lax.all_gather(tokens, 'tp', axis_index_groups=same_core)  13.3 us
    all_to_all x1, blocking collectives, per_device(): lax.all_to_all(partial.reshape(tp // 2, -1, partial.shape[1]), 'tp', 0, 0...  12.9 us
    pallas_call x1, Pallas kernels, attend(): pl.pallas_call(functools.partial(attend_kernel, chunk, span), grid=(count...  12.1 us
    all_to_all x1, starting transfers between devices, per_device(): lax.all_to_all(parts, 'sp', 0, 0, axis_index_groups=near, tiled=True)  11.2 us
    ppermute x1, waiting for transfers between devices, earlier_blocks(): lax.ppermute(shifted, 'sp', [(i, i + chunk) for i in range(devices - chun...  6.65 us
    all_to_all x1, waiting for transfers between devices, per_device(): lax.all_to_all(parts, 'sp', 0, 0, axis_index_groups=near, tiled=True)  5.96 us
    all_to_all x1, starting transfers between devices, per_device(): lax.all_to_all(query, 'sp', 0, 0, axis_index_groups=near, tiled=True)  5.92 us
  transfers between devices with their start and end apart: 5, of which 4 were waited for; matrix products, arithmetic and copies ran while one was open for 0% of the time, Pallas kernels for 3%

profile of v6, /device:TPU:480, one launch (start us, length us, event | category | flops | bytes accessed | tf_op | source)
XLA Modules:
  0.0 123.9 jit_solution(54658473527666774)
XLA Ops:
  0.6 13.3 %all-gather = bf16[1024,256]{1,0:T(8,128)(2,1)S(1)} all-gather(bf16[256,256]{1,0:T(8,128)(2,1)} %param.14), channel_id=2, replica_groups={{0,2,4,6},{1,3,5,7},{8,10,12,14},{9,11,13,15},{16,18,20,22},{17,19,21,2..., dimensions={0}, use_global_device_ids=true | all-gather | bytes 655360 | tf_op jit(solution)/shard_map/all_gather | solution.py:339
  14.0 1.9 %collective-permute-start = (bf16[4,256,256]{2,1,0:T(8,128)(2,1)S(1)}, bf16[4,256,256]{2,1,0:T(8,128)(2,1)S(1)}, u32[]{:S(2)}, u32[]{:S(2)}) collective-permute-start(bf16[4,256,256]{2,1,0:T(8,128)(2,1)S(1)} %bitcast.6), channel_id=1, source_target_pairs={{0,1},{1,0},{2,3},{3,2},{4,5},{5,4},{6,7},{7,6},{8,9},{9,8},{10,11... | collective-permute-start | bytes 1572872 | tf_op jit(solution)/shard_map/ppermute | solution.py:340
  15.9 1.9 %collective-permute-done.other = bf16[4,256,256]{2,1,0:T(8,128)(2,1)S(1)} collective-permute-done((bf16[4,256,256]{2,1,0:T(8,128)(2,1)S(1)}, bf16[4,256,256]{2,1,0:T(8,128)(2,1)S(1)}, u32[]{:S(2)}, u32[]{:S(2)}) %collective-permute-start) | collective-permute-done | bytes 524320 | tf_op jit(solution)/shard_map/ppermute | solution.py:340
  17.8 4.2 %project.1 = (bf16[256,256]{1,0:T(8,128)(2,1)S(1)}, bf16[240,256]{1,0:T(8,128)(2,1)S(1)}, bf16[8,256,128]{2,1,0:T(8,128)(2,1)}, bf16[256,2048]{1,0:T(8,128)(2,1)}, f32[256,128]{1,0:T(8,128)}) custom-call(bf16[4,256,256]{2,1,0:T(8,128)(2,1)S(1)} %bitcast.7, f32[1,2048]{1,0:T(1,128)} %bitcast.9, bf16[2048,128]{1,0:T(8,128)(2,1)} %qw.1, bf16[2048,128]{1,0:T(8,128)(2,1)} %kw.1, ...), custom_call_target="tpu_custom_call" | custom-call | tf_op jit(solution)/shard_map/project/pallas_call | solution.py:232
  21.9 5.9 %all-to-all-start = ((bf16[8,256,128]{2,1,0:T(8,128)(2,1)}), bf16[8,256,128]{2,1,0:T(8,128)(2,1)S(1)}, u32[]{:S(2)}, u32[]{:S(2)}) async-start(bf16[8,256,128]{2,1,0:T(8,128)(2,1)} %get-tuple-element.16), calls=%async_computation | async-start | bytes 1048576 | tf_op jit(solution)/shard_map/all_to_all | solution.py:350
  27.9 1.3 %collective-permute-start.1 = (bf16[240,256]{1,0:T(8,128)(2,1)S(1)}, bf16[240,256]{1,0:T(8,128)(2,1)S(1)}, u32[]{:S(2)}, u32[]{:S(2)}) collective-permute-start(bf16[240,256]{1,0:T(8,128)(2,1)S(1)} %get-tuple-element.18.ending), channel_id=1, source_target_pairs={{0,64},{8,72},{16,80},{24,88},{32,96},{40,104},{48,112},{56,120},{... | collective-permute-start | bytes 368648 | tf_op jit(solution)/shard_map/ppermute | solution.py:309
  29.2 6.7 %collective-permute-done.1.moved = bf16[240,256]{1,0:T(8,128)(2,1)S(1)} collective-permute-done((bf16[240,256]{1,0:T(8,128)(2,1)S(1)}, bf16[240,256]{1,0:T(8,128)(2,1)S(1)}, u32[]{:S(2)}, u32[]{:S(2)}) %collective-permute-start.1) | collective-permute-done | bytes 122912 | tf_op jit(solution)/shard_map/ppermute | solution.py:309
  35.8 0.3 fusion
  36.1 32.0 %all_gather.11 = bf16[1792,256]{1,0:T(8,128)(2,1)S(1)} all-gather(bf16[224,256]{1,0:T(8,128)(2,1)S(1)} %fusion), channel_id=1, replica_groups={{0,64,128,192,256,320,384,448},{8,72,136,200,264,328,392,456},{16,80,14..., dimensions={0}, use_global_device_ids=true | all-gather | bytes 1032192 | tf_op jit(solution)/shard_map/all_gather | solution.py:312
  68.1 0.0 all-to-all-done.q
  68.1 12.1 %attend.1 = bf16[8,272,256]{2,1,0:T(8,128)(2,1)} custom-call(bf16[8,256,128]{2,1,0:T(8,128)(2,1)S(1)} %all-to-all-done.q, bf16[256,256]{1,0:T(8,128)(2,1)S(1)} %get-tuple-element.17.own, bf16[240,256]{1,0:T(8,128)(2,1)S(1)} %get-tuple-element.18.ending, bf16[240,256]{1,0:T(8,128)(2,1)S(1)} %collective-permute-done.1.moved, bf16[7,256,256]{2,1,0:T(8,128)(2,1)S(1)} %bitcast.5), custom_call_target="tpu_custom_call" | custom-call | tf_op jit(solution)/shard_map/attend/pallas_call | solution.py:267
  80.2 11.2 %all-to-all-start.1 = ((bf16[8,272,256]{2,1,0:T(8,128)(2,1)}), bf16[8,272,256]{2,1,0:T(8,128)(2,1)S(1)}, u32[]{:S(2)}, u32[]{:S(2)}) async-start(bf16[8,272,256]{2,1,0:T(8,128)(2,1)} %attend.1), calls=%async_computation.1 | async-start | bytes 2228224 | tf_op jit(solution)/shard_map/all_to_all | solution.py:355
  92.0 3.8 %gates.1 = (bf16[256,128]{1,0:T(8,128)(2,1)}, bf16[256,128]{1,0:T(8,128)(2,1)}, bf16[256,128]{1,0:T(8,128)(2,1)}) custom-call(bf16[256,2048]{1,0:T(8,128)(2,1)} %get-tuple-element.19.normed, f32[256,128]{1,0:T(8,128)} %get-tuple-element.20.scale, bf16[2048,128]{1,0:T(8,128)(2,1)} %gw.1, bf16[2048,128]{1,0:T(8,128)(2,1)} %ow.1, bf16[2048,128]{1,0:T(8,128)(2,1)} %iw.3, ...), custom_call_target="tpu_custom_call" | custom-call | flops 536870912 | bytes 2097152 | tf_op jit(solution)/shard_map/gates/pallas_call | solution.py:249
  95.8 6.0 %all-to-all-done.1.parts = bf16[8,272,256]{2,1,0:T(8,128)(2,1)S(1)} async-done(((bf16[8,272,256]{2,1,0:T(8,128)(2,1)}), bf16[8,272,256]{2,1,0:T(8,128)(2,1)S(1)}, u32[]{:S(2)}, u32[]{:S(2)}) %all-to-all-start.1) | async-done | bytes 1114144 | tf_op jit(solution)/shard_map/all_to_all | solution.py:355
  101.8 3.0 %finish.1 = (bf16[128,2048]{1,0:T(8,128)(2,1)S(1)}, bf16[128,256]{1,0:T(8,128)(2,1)S(1)}, f32[1,2,256]{2,1,0:T(2,128)}) custom-call(f32[1]{0:T(128)S(6)} %copy.16.lam, bf16[256,128]{1,0:T(8,128)(2,1)} %get-tuple-element.21.gate, bf16[256,128]{1,0:T(8,128)(2,1)} %get-tuple-element.22.outer, bf16[256,128]{1,0:T(8,128)(2,1)} %get-tuple-element.23.insig, ...), custom_call_target="tpu_custom_call" | custom-call | tf_op jit(solution)/shard_map/finish/pallas_call | solution.py:280
  104.8 1.9 %collective-permute-start.2 = (bf16[128,2048]{1,0:T(8,128)(2,1)S(1)}, bf16[128,2048]{1,0:T(8,128)(2,1)S(1)}, u32[]{:S(2)}, u32[]{:S(2)}) collective-permute-start(bf16[128,2048]{1,0:T(8,128)(2,1)S(1)} %get-tuple-element.26), channel_id=1, source_target_pairs={{0,1},{1,0},{2,3},{3,2},{4,5},{5,4},{6,7},{7,6},{8,9},{9,8},{10,11... | collective-permute-start | bytes 1572872 | tf_op jit(solution)/shard_map/ppermute | solution.py:359
  106.7 1.9 %collective-permute-done.2.received = bf16[128,2048]{1,0:T(8,128)(2,1)S(1)} collective-permute-done((bf16[128,2048]{1,0:T(8,128)(2,1)S(1)}, bf16[128,2048]{1,0:T(8,128)(2,1)S(1)}, u32[]{:S(2)}, u32[]{:S(2)}) %collective-permute-start.2) | collective-permute-done | bytes 524320 | tf_op jit(solution)/shard_map/ppermute | solution.py:359
  108.6 1.6 %join.1 = bf16[128,2048]{1,0:T(8,128)(2,1)S(1)} custom-call(bf16[128,256]{1,0:T(8,128)(2,1)S(1)} %get-tuple-element.25.kept, bf16[128,2048]{1,0:T(8,128)(2,1)S(1)} %collective-permute-done.2.received, bf16[128,2048]{1,0:T(8,128)(2,1)} %attn_w.3, bf16[128,2048]{1,0:T(8,128)(2,1)} %conv_w.3), custom_call_target="tpu_custom_call" | custom-call | tf_op jit(solution)/shard_map/join/pallas_call | solution.py:294
  110.2 12.9 %all_to_all.15 = bf16[4,32,2048]{2,1,0:T(8,128)(2,1)S(1)} all-to-all(bf16[4,32,2048]{2,1,0:T(8,128)(2,1)S(1)} %bitcast.8), channel_id=1, replica_groups={{0,2,4,6},{1,3,5,7},{8,10,12,14},{9,11,13,15},{16,18,20,22},{17,19,21,2..., dimensions={0} | all-to-all | bytes 1048576 | tf_op jit(solution)/shard_map/all_to_all | solution.py:361
  123.1 0.7 reduce_sum.12
  (1 shorter events, 0.0 us)
Async XLA Ops:
  14.0 3.8 %collective-permute-start = (bf16[4,256,256]{2,1,0:T(8,128)(2,1)S(1)}, bf16[4,256,256]{2,1,0:T(8,128)(2,1)S(1)}, u32[]{:S(2)}, u32[]{:S(2)}) collective-permute-start(bf16[4,256,256]{2,1,0:T(8,128)(2,1)S(1)} %bitcast.6), channel_id=1, source_target_pairs={{0,1},{1,0},{2,3},{3,2},{4,5},{5,4},{6,7},{7,6},{8,9},{9,8},{10,11... | collective-permute-start | bytes 1572872 | tf_op jit(solution)/shard_map/ppermute | solution.py:340
  21.9 46.2 %all-to-all-start = ((bf16[8,256,128]{2,1,0:T(8,128)(2,1)}), bf16[8,256,128]{2,1,0:T(8,128)(2,1)S(1)}, u32[]{:S(2)}, u32[]{:S(2)}) async-start(bf16[8,256,128]{2,1,0:T(8,128)(2,1)} %get-tuple-element.16), calls=%async_computation | async-start | bytes 1048576 | tf_op jit(solution)/shard_map/all_to_all | solution.py:350
  27.9 7.9 %collective-permute-start.1 = (bf16[240,256]{1,0:T(8,128)(2,1)S(1)}, bf16[240,256]{1,0:T(8,128)(2,1)S(1)}, u32[]{:S(2)}, u32[]{:S(2)}) collective-permute-start(bf16[240,256]{1,0:T(8,128)(2,1)S(1)} %get-tuple-element.18.ending), channel_id=1, source_target_pairs={{0,64},{8,72},{16,80},{24,88},{32,96},{40,104},{48,112},{56,120},{... | collective-permute-start | bytes 368648 | tf_op jit(solution)/shard_map/ppermute | solution.py:309
  80.2 21.5 %all-to-all-start.1 = ((bf16[8,272,256]{2,1,0:T(8,128)(2,1)}), bf16[8,272,256]{2,1,0:T(8,128)(2,1)S(1)}, u32[]{:S(2)}, u32[]{:S(2)}) async-start(bf16[8,272,256]{2,1,0:T(8,128)(2,1)} %attend.1), calls=%async_computation.1 | async-start | bytes 2228224 | tf_op jit(solution)/shard_map/all_to_all | solution.py:355
  104.8 3.8 %collective-permute-start.2 = (bf16[128,2048]{1,0:T(8,128)(2,1)S(1)}, bf16[128,2048]{1,0:T(8,128)(2,1)S(1)}, u32[]{:S(2)}, u32[]{:S(2)}) collective-permute-start(bf16[128,2048]{1,0:T(8,128)(2,1)S(1)} %get-tuple-element.26), channel_id=1, source_target_pairs={{0,1},{1,0},{2,3},{3,2},{4,5},{5,4},{6,7},{7,6},{8,9},{9,8},{10,11... | collective-permute-start | bytes 1572872 | tf_op jit(solution)/shard_map/ppermute | solution.py:359
